TPU v7x, 32 devices: a whole 2x2x4 slice. The times are simulated.
32 devices in a mesh: sp: 8 (over z, x), tp: 4 (over y, core).
Axes of the slice: x: 2, y: 2, z: 4, core: 2. Of those that a mesh axis runs over, the one named last changes fastest.
Arguments:
- stratum_source_matrix: bfloat16 [1024, 2048], P('sp'), may hold values from -70 to 70
- acceptance_query: bfloat16 [2, 1024, 1024], P(None, 'sp', 'tp'), may hold values from -6 to 6
- cluster_lookup_matrix: bfloat16 [2, 1024, 1024], P(None, 'sp', 'tp'), may hold values from -6 to 6
- cluster_payload_matrix: bfloat16 [2, 1024, 1024], P(None, 'sp', 'tp'), may hold values from -6 to 6
- fading_logit: bfloat16 [2, 1024, 1024], P(None, 'sp', 'tp'), may hold values from -17 to 2
- adaptation_speed_logit: bfloat16 [2, 1024, 1024], P(None, 'sp', 'tp'), may hold values from -14 to 5
- additional_fading_exponent: float32 [2, 1024, 1024], P(None, 'sp', 'tp'), may hold values from -0.7 to 0
- result_switch_pair: bfloat16 [2, 1024, 1024], P(None, 'sp', 'tp'), may hold values from -6 to 6
- attender_scaling_factor: float32 [2, 1024], P(None, 'tp'), may hold values from 0.1 to 1.9
- present_item_factor: float32 [2, 1024], P(None, 'tp'), may hold values from -0.9 to 0.9
- final_mapping_matrix: bfloat16 [2, 1024, 2048], P(None, 'tp'), may hold values from -0.125 to 0.125
- perceptron_scaling_factor: float32 [2048], replicated, may hold values from 0.1 to 1.9
- switching_matrix: bfloat16 [2048, 5632], P('sp', 'tp'), may hold values from -0.125 to 0.125
- widening_matrix: bfloat16 [2048, 5632], P('sp', 'tp'), may hold values from -0.125 to 0.125
- shrinking_matrix: bfloat16 [5632, 2048], P('tp', 'sp'), may hold values from -0.078125 to 0.078125
Outputs:
- layer_out: bfloat16 [1024, 2048], P('sp', 'tp')
All inputs are finite; a program needn't handle non-finite values.
Results may differ from a plain program's by a relative error of at most 0.014.
Values may be sent and summed in bfloat16 or wider, within the bound.
A program may use at most 128 MiB of HBM per device.

v0:
```python
import functools

import jax
import jax.numpy as jnp
from jax import lax
from jax.experimental import pallas as pl
from jax.experimental.pallas import tpu as pltpu
from jax.sharding import PartitionSpec as P

DS = 64
DL = 128
LANES = 128
MESH = pl.DeviceIdType.MESH

norm_epsilon = 1e-06
head_epsilon = 0.00064
key_epsilon = 1e-06


NN = (((1,), (0,)), ((), ()))
NT = (((1,), (1,)), ((), ()))


def split(x, count=2):
    if x.dtype == jnp.bfloat16:
        return [x]
    parts = []
    for _ in range(count - 1):
        high = x.astype(jnp.bfloat16)
        parts.append(high)
        x = x - high.astype(jnp.float32)
    return parts + [x.astype(jnp.bfloat16)]


def product(a, b, dims, count=2):
    total = None
    for i, p in enumerate(split(a, count)):
        for j, r in enumerate(split(b, count)):
            if i + j < count:
                term = lax.dot_general(p, r, dims, preferred_element_type=jnp.float32)
                total = term if total is None else total + term
    return total


def mm(a, b, count=2):
    return product(a, b, NN, count)


def mm_nt(a, b):
    return product(a, b, NT)


def sigmoid(x):
    return 1.0 / (1.0 + jnp.exp(-x))


def same_head(width):
    i = lax.broadcasted_iota(jnp.int32, (LANES, LANES), 0) // width
    j = lax.broadcasted_iota(jnp.int32, (LANES, LANES), 1) // width
    return (i == j).astype(jnp.float32).astype(jnp.bfloat16)


def unit_inverse(strict_part, rows, cols):
    size = strict_part.shape[0]
    inverse = (rows == cols).astype(jnp.float32)
    half = 1
    while half < size:
        off = (rows // (2 * half) == cols // (2 * half)) & (rows // half != cols // half)
        part = jnp.where(off, strict_part, 0.0)
        if half == 1:
            inverse = inverse + part
        else:
            inverse = inverse + mm(mm(inverse, part), inverse)
        half *= 2
    return inverse


def local_unit(width, q, k, v, fade, speed, extra):
    T = q.shape[0]
    ones = same_head(width)
    log_decay = extra - jnp.exp(jnp.float32(-0.5)) * sigmoid(fade)
    removal = k * lax.rsqrt(mm(k * k, ones) + key_epsilon)
    left = -removal
    right = sigmoid(speed) * removal
    rows = lax.broadcasted_iota(jnp.int32, (T, T), 0)
    cols = lax.broadcasted_iota(jnp.int32, (T, T), 1)
    inclusive = rows >= cols
    strict = rows > cols
    cumulative = mm(inclusive.astype(jnp.float32).astype(jnp.bfloat16), log_decay, 3)
    middle = cumulative[T // 2 : T // 2 + 1, :]
    final = cumulative[T - 1 : T, :]
    forward = jnp.exp(cumulative - middle)
    backward = jnp.exp(middle - cumulative)
    tail = jnp.exp(final - cumulative)
    queries = jnp.concatenate([left * jnp.exp(-log_decay) * forward, q * forward], axis=0)
    sources = jnp.concatenate([right * backward, k * backward], axis=0)
    start_target = left * jnp.exp(cumulative - log_decay)
    right_tail = right * tail
    key_tail = k * tail
    eye = lax.broadcasted_iota(jnp.int32, (LANES, LANES), 0) == lax.broadcasted_iota(
        jnp.int32, (LANES, LANES), 1
    )
    transit = jnp.where(eye, jnp.exp(final), 0.0)
    start_read = q * jnp.exp(cumulative)
    added = jnp.zeros((LANES, LANES), jnp.float32)
    local_out = jnp.zeros((T, LANES), jnp.float32)
    lane = lax.broadcasted_iota(jnp.int32, (1, LANES), 1) // width
    for head in range(LANES // width):
        only = lane == head
        pick = (lambda a: a) if width == LANES else (lambda a: jnp.where(only, a, 0.0))
        pairs = mm_nt(pick(queries), sources)
        remove_remove = jnp.where(strict, pairs[:T, :T], 0.0)
        remove_key = jnp.where(strict, pairs[:T, T:], 0.0)
        read_remove = jnp.where(inclusive, pairs[T:, :T], 0.0)
        read_key = jnp.where(inclusive, pairs[T:, T:], 0.0)
        inverse = unit_inverse(remove_remove, rows, cols)
        value = pick(v)
        carried = mm(inverse, mm(remove_key, value))
        start = mm(inverse, pick(start_target))
        local_out = local_out + mm(read_remove, carried) + mm(read_key, value)
        start_read = start_read + mm(read_remove, start)
        head_right = pick(right_tail)
        transit = transit + mm(start.T, head_right)
        added = added + mm(carried.T, head_right) + mm(value.T, pick(key_tail))
    return local_out, start_read, transit, added


def finish_unit(width, read, q, k, v, gain, own, gate):
    ones = same_head(width)
    mean = mm(read, ones) / width
    centered = read - mean
    variance = mm(centered * centered, ones) / width
    normed = centered * lax.rsqrt(variance + head_epsilon) * gain
    diagonal = mm(q * k * own, ones) * v
    return ((normed + diagonal) * gate).astype(jnp.bfloat16)


def attention_kernel(
    n_sp, widths, q_ref, k_ref, v_ref, f_ref, a_ref, e_ref, g_ref, gain_ref, own_ref,
    first_ref, second_ref, mixed_ref, first_out, second_out,
    local_ref, read_ref, mine, got, send_sem, recv_sem,
    up_sem, down_sem, along_sem, side_sem, side_recv, keep_sem,
):
    me = lax.axis_index("sp")
    tp = lax.axis_index("tp")

    barrier = pltpu.get_barrier_semaphore()

    @pl.loop(1, n_sp)
    def _(d):
        pl.semaphore_signal(
            barrier, inc=1, device_id=(lax.rem(me + d, n_sp), tp), device_id_type=MESH
        )

    pl.semaphore_wait(barrier, n_sp - 1)

    line, side = me // 2, me % 2
    length = n_sp // 2
    weights = ((first_ref, first_out), (second_ref, second_out))

    def pass_on(w, block, to, source, sem, landed):
        return pltpu.make_async_remote_copy(
            src_ref=source, dst_ref=weights[w][1].at[block], send_sem=sem, recv_sem=landed,
            device_id=(to, tp), device_id_type=MESH,
        )

    def to_line(w, at, to, source, sem):
        return pass_on(w, at * 2 + side, to * 2 + side, source, sem.at[w, at], along_sem.at[w, at])

    def to_side(w, at, source):
        return pass_on(
            w, at * 2 + side, line * 2 + 1 - side, source, side_sem.at[w, at], side_recv.at[w, at]
        )

    def spread(w, at, source, upward, downward):
        if upward:

            @pl.when(line + 1 < length)
            def _():
                to_line(w, at, line + 1, source, up_sem).start()

        if downward:

            @pl.when(line >= 1)
            def _():
                to_line(w, at, line - 1, source, down_sem).start()

        to_side(w, at, source).start()

    def relay(i):
        for w in range(2):
            below, above = line - i, line + i

            @pl.when(below >= 0)
            def _():
                source = weights[w][1].at[below * 2 + side]
                to_line(w, below, line, source, up_sem).wait_recv()
                spread(w, below, source, True, False)

            @pl.when(above < length)
            def _():
                source = weights[w][1].at[above * 2 + side]
                to_line(w, above, line, source, down_sem).wait_recv()
                spread(w, above, source, False, True)

    for w in range(2):
        spread(w, line, weights[w][0], True, True)
    keeps = [
        pltpu.make_async_copy(weights[w][0], weights[w][1].at[me], keep_sem.at[w])
        for w in range(2)
    ]
    for keep in keeps:
        keep.start()

    per_group = q_ref.shape[2] // LANES

    def load(ref, g, c):
        return ref[g, :, c * LANES : (c + 1) * LANES].astype(jnp.float32)

    def copy(u, d, to):
        return pltpu.make_async_remote_copy(
            src_ref=mine.at[u],
            dst_ref=got.at[d, u],
            send_sem=send_sem.at[u, d],
            recv_sem=recv_sem.at[u, d],
            device_id=(to, tp),
            device_id_type=MESH,
        )

    units = [(g, c) for g in range(2) for c in range(per_group)]
    for u, (g, c) in enumerate(units):
        local_out, start_read, transit, added = local_unit(
            widths[g], *(load(r, g, c) for r in (q_ref, k_ref, v_ref, f_ref, a_ref, e_ref))
        )
        local_ref[u] = local_out
        read_ref[u] = start_read
        mine[u, 0] = transit.astype(jnp.bfloat16)
        mine[u, 1] = added.astype(jnp.bfloat16)

        @pl.loop(1, n_sp)
        def _(d):
            @pl.when(me + d < n_sp)
            def _():
                copy(u, d, me + d).start()

        if u == 1 and length > 1:
            relay(1)
        if u == 3 and length > 2:
            relay(2)

    for u in range(len(units)):

        @pl.loop(1, n_sp)
        def _(d):
            @pl.when(me - d >= 0)
            def _():
                copy(u, d, me).wait_recv()

    def fold(step, states):
        d = me - step
        return tuple(
            mm(s, got[d, u, 0]) + got[d, u, 1].astype(jnp.float32)
            for u, s in enumerate(states)
        )

    states = lax.fori_loop(
        0, me, fold, tuple(jnp.zeros((LANES, LANES), jnp.float32) for _ in units)
    )
    for u, (g, c) in enumerate(units):
        lanes = slice(c * LANES, (c + 1) * LANES)
        read = local_ref[u] + mm_nt(read_ref[u], states[u])
        mixed = finish_unit(
            widths[g], read, load(q_ref, g, c), load(k_ref, g, c), load(v_ref, g, c),
            gain_ref[g : g + 1, lanes], own_ref[g : g + 1, lanes], load(g_ref, g, c),
        )
        mixed_ref[:, u * LANES : (u + 1) * LANES] = mixed

    for i in range(3, length):
        relay(i)

    for keep in keeps:
        keep.wait()

    @pl.loop(0, length)
    def _(at):
        for w in range(2):
            source = weights[w][0]
            to_side(w, at, source).wait()

            @pl.when((at <= line) & (line + 1 < length))
            def _():
                to_line(w, at, line + 1, source, up_sem).wait_send()

            @pl.when((at >= line) & (line >= 1))
            def _():
                to_line(w, at, line - 1, source, down_sem).wait_send()

    for u in range(len(units)):

        @pl.loop(1, n_sp)
        def _(d):
            @pl.when(me + d < n_sp)
            def _():
                copy(u, d, me + d).wait_send()


def attention(n_sp, q, k, v, f, a, e, g, gain, own, first, second):
    T, channels = q.shape[1], q.shape[2]
    units = 2 * channels // LANES
    vmem = pl.BlockSpec(memory_space=pltpu.VMEM)
    return pl.pallas_call(
        functools.partial(attention_kernel, n_sp, (DS, DL)),
        out_shape=[
            jax.ShapeDtypeStruct((T, 2 * channels), jnp.bfloat16),
            jax.ShapeDtypeStruct((n_sp,) + first.shape, first.dtype),
            jax.ShapeDtypeStruct((n_sp,) + second.shape, second.dtype),
        ],
        in_specs=[vmem] * 11,
        out_specs=[vmem, pl.BlockSpec(memory_space=pl.ANY), pl.BlockSpec(memory_space=pl.ANY)],
        scratch_shapes=[
            pltpu.VMEM((units, T, LANES), jnp.float32),
            pltpu.VMEM((units, T, LANES), jnp.float32),
            pltpu.VMEM((units, 2, LANES, LANES), jnp.bfloat16),
            pltpu.VMEM((n_sp, units, 2, LANES, LANES), jnp.bfloat16),
            pltpu.SemaphoreType.DMA((units, n_sp)),
            pltpu.SemaphoreType.DMA((units, n_sp)),
        ]
        + [pltpu.SemaphoreType.DMA((2, n_sp // 2))] * 5
        + [pltpu.SemaphoreType.DMA((2,))],
        compiler_params=pltpu.CompilerParams(
            collective_id=0, has_side_effects=True, vmem_limit_bytes=60 * 2**20
        ),
        cost_estimate=pl.CostEstimate(
            flops=15 * 10**10, bytes_accessed=2**28, transcendentals=0
        ),
        name="attention",
    )(q, k, v, f, a, e, g, gain, own, first, second)


def on_device(
    stratum_source_matrix,
    acceptance_query,
    cluster_lookup_matrix,
    cluster_payload_matrix,
    fading_logit,
    adaptation_speed_logit,
    additional_fading_exponent,
    result_switch_pair,
    attender_scaling_factor,
    present_item_factor,
    final_mapping_matrix,
    perceptron_scaling_factor,
    switching_matrix,
    widening_matrix,
    shrinking_matrix,
):
    down_whole = lax.all_gather(shrinking_matrix, "sp", axis=1, tiled=True)
    mixed, gate_whole, up_whole = attention(
        lax.axis_size("sp"),
        acceptance_query,
        cluster_lookup_matrix,
        cluster_payload_matrix,
        fading_logit,
        adaptation_speed_logit,
        additional_fading_exponent,
        result_switch_pair,
        attender_scaling_factor,
        present_item_factor,
        switching_matrix,
        widening_matrix,
    )
    gate_whole = gate_whole.reshape(-1, gate_whole.shape[2])
    up_whole = up_whole.reshape(-1, up_whole.shape[2])
    partial_value = jnp.dot(
        mixed,
        final_mapping_matrix.reshape(-1, final_mapping_matrix.shape[2]),
        preferred_element_type=jnp.float32,
    )
    columns = perceptron_scaling_factor.shape[0] // lax.axis_size("tp")
    own_start = lax.axis_index("tp") * columns
    residual_float = stratum_source_matrix.astype(jnp.float32)
    branch = lax.psum_scatter(
        partial_value.astype(jnp.bfloat16), "tp", scatter_dimension=1, tiled=True
    ).astype(jnp.float32)
    own_residual = lax.dynamic_slice_in_dim(residual_float, own_start, columns, 1)
    own_state = (own_residual + branch).astype(jnp.bfloat16).astype(jnp.float32)
    square_total = lax.psum(jnp.sum(own_state * own_state, axis=1), "tp")
    own_gain = lax.dynamic_slice_in_dim(perceptron_scaling_factor, own_start, columns, 0)
    scaled = (
        own_state
        * lax.rsqrt(square_total / perceptron_scaling_factor.shape[0] + norm_epsilon)[:, None]
        * own_gain
    )
    normed = lax.all_gather(scaled.astype(jnp.bfloat16), "tp", axis=1, tiled=True)
    gate_pre = jnp.dot(normed, gate_whole, preferred_element_type=jnp.float32)
    up_pre = jnp.dot(normed, up_whole, preferred_element_type=jnp.float32)
    activated = (jax.nn.silu(gate_pre) * up_pre).astype(jnp.bfloat16)
    down_terms = jnp.dot(
        activated,
        down_whole,
        preferred_element_type=jnp.float32,
    )
    mixer = lax.psum_scatter(
        down_terms.astype(jnp.bfloat16), "tp", scatter_dimension=1, tiled=True
    ).astype(jnp.float32)
    return (own_state + mixer).astype(jnp.bfloat16)


def solution(mesh):
    tokens = P(None, "sp", "tp")
    in_specs = (
        P("sp", None), tokens, tokens, tokens, tokens, tokens, tokens, tokens,
        P(None, "tp"), P(None, "tp"), P(None, "tp", None), P(),
        P("sp", "tp"), P("sp", "tp"), P("tp", "sp"),
    )
    return jax.shard_map(
        on_device, mesh=mesh, in_specs=in_specs, out_specs=P("sp", "tp"), check_vma=False
    )
```

profile of v0, /device:TPU:0, one launch (start us, length us, event | category | flops | bytes accessed | tf_op | source)
XLA Modules:
  0.0 296.2 jit_solution(5747960441052812434)
XLA Ops:
  7.4 0.0 copy-start
  7.4 0.0 reduce-scatter.3.cloned.1.call-start
  7.4 139.0 %attention.1 = (bf16[128,512]{1,0:T(8,128)(2,1)}, bf16[8,256,1408]{2,1,0:T(8,128)(2,1)}, bf16[8,256,1408]{2,1,0:T(8,128)(2,1)}) custom-call(bf16[2,128,256]{2,1,0:T(8,128)(2,1)} %q_ref.1, bf16[2,128,256]{2,1,0:T(8,128)(2,1)} %k_ref.1, bf16[2,128,256]{2,1,0:T(8,128)(2,1)} %v_ref.1, bf16[2,128,256]{2,1,0:T(8,128)(2,1)} %f_ref.1, bf16[2,128,256]{2,1,0:T(8,128)(2,1)} %a_ref.1, ...), custom_call_target="tpu_custom_call" | custom-call | flops 149999992832 | bytes 268435456 | tf_op jit(solution)/shard_map/attention/pallas_call | solution.py:311
  146.3 0.0 copy-done
  146.3 2.2 convolution_convert_fusion
  148.5 0.0 reduce-scatter.3.cloned.1.call-update
  148.5 0.0 all-gather.2.cloned.1.call-start
  148.6 0.5 all-gather.2.cloned.1.call-update
  149.1 0.0 reduce-scatter.5.cloned.1.call-start
  149.2 0.8 dynamic_slice.7
  149.9 36.6 %reduce-scatter.3.cloned.1.call-done = bf16[128,512]{1,0:T(8,128)(2,1)} async-done(((bf16[128,2048]{1,0:T(8,128)(2,1)}), bf16[128,512]{1,0:T(8,128)(2,1)}) %reduce-scatter.3.cloned.1.call-update) | async-done | bytes 131088 | tf_op jit(solution)/shard_map/reduce_scatter | solution.py:382
  186.5 1.1 fusion.2
  187.6 6.1 %psum.7 = f32[128]{0:T(128)S(1)} all-reduce(f32[128]{0:T(128)S(1)} %get-tuple-element.11), channel_id=1, replica_groups=mesh['sp'=8,'tp'=4] {'tp'}, use_global_device_ids=true, to_apply=%region_2.0 | all-reduce | flops 128 | bytes 1024 | tf_op jit(solution)/shard_map/psum | solution.py:387
  193.7 0.1 fusion.4
  193.8 7.2 %all_gather.6 = bf16[128,2048]{1,0:T(8,128)(2,1)S(1)} all-gather(bf16[128,512]{1,0:T(8,128)(2,1)S(1)} %fusion.4), channel_id=1, replica_groups=mesh['sp'=8,'tp'=4] {'tp'}, dimensions={1}, use_global_device_ids=true | all-gather | bytes 655360 | tf_op jit(solution)/shard_map/all_gather | solution.py:394
  200.9 3.6 %fusion.7 = f32[128,1408]{1,0:T(8,128)S(1)} fusion(bf16[128,2048]{1,0:T(8,128)(2,1)S(1)} %all_gather.6, bf16[2048,1408]{1,0:T(8,128)(2,1)} %bitcast.11), kind=kOutput, calls=%fused_computation.15 | convolution fusion | flops 738197504 | bytes 7012352 | tf_op jit(solution)/shard_map/dot_general | solution.py:395
  204.6 55.5 %all-gather.2.cloned.1.call-done = bf16[1408,2048]{1,0:T(8,128)(2,1)} async-done(((bf16[1408,256]{1,0:T(8,128)(2,1)}), bf16[1408,2048]{1,0:T(8,128)(2,1)}) %all-gather.2.cloned.1.call-update) | async-done | bytes 5767184 | tf_op jit(solution)/shard_map/all_gather | solution.py:357
  260.1 7.1 %convolution_convert_fusion.1 = bf16[128,2048]{1,0:T(8,128)(2,1)} fusion(bf16[1408,2048]{1,0:T(8,128)(2,1)} %all-gather.2.cloned.1.call-done, bf16[128,2048]{1,0:T(8,128)(2,1)S(1)} %all_gather.6, bf16[2048,1408]{1,0:T(8,128)(2,1)} %bitcast.12, f32[128,1408]{1,0:T(8,128)S(1)} %fusion.7), kind=kOutput, calls=%fused_computation.3 | convolution fusion | flops 1477738496 | bytes 13303808 | tf_op jit(solution)/shard_map/dot_general | solution.py:398
  267.2 0.0 reduce-scatter.5.cloned.1.call-update
  267.2 20.0 %reduce-scatter.5.cloned.1.call-done = bf16[128,512]{1,0:T(8,128)(2,1)} async-done(((bf16[128,2048]{1,0:T(8,128)(2,1)}), bf16[128,512]{1,0:T(8,128)(2,1)}) %reduce-scatter.5.cloned.1.call-update) | async-done | bytes 131088 | tf_op jit(solution)/shard_map/reduce_scatter | solution.py:403
  287.2 1.6 fusion.5
  (1 shorter events, 0.0 us)
Async XLA Ops:
  7.4 139.0 %copy-start = (bf16[2,256,2048]{2,1,0:T(8,128)(2,1)S(1)}, bf16[2,256,2048]{2,1,0:T(8,128)(2,1)}, u32[]{:S(2)}) copy-start(bf16[2,256,2048]{2,1,0:T(8,128)(2,1)} %param.25) | copy-start | bytes 6291460
  7.4 179.1 %reduce-scatter.3.cloned.1.call-start = ((), (), s32[]{:S(2)}) async-start(), calls=%async_computation.2 | async-start | bytes 655360 | tf_op jit(solution)/shard_map/reduce_scatter | solution.py:382
  148.5 111.6 %all-gather.2.cloned.1.call-start = ((), (), s32[]{:S(2)}) async-start(), calls=%async_computation.3 | async-start | bytes 6488064 | tf_op jit(solution)/shard_map/all_gather | solution.py:357
  149.1 138.1 %reduce-scatter.5.cloned.1.call-start = ((), (), s32[]{:S(2)}) async-start(), calls=%async_computation.4 | async-start | bytes 655360 | tf_op jit(solution)/shard_map/reduce_scatter | solution.py:403
Sparse Core Ops, SparseCore 0:
  148.7 37.7 reduce-scatter.2
  267.3 19.8 reduce-scatter.4
Sparse Core Ops, SparseCore 1:
  151.1 109.0 all-gather.1
where the time goes:
time: 296 us
  Pallas kernels  139 us (47%)
  waiting for transfers between devices  113 us (38%)
  between operations  14.9 us (5%)
  blocking collectives  13.2 us (4%)
  matrix products  12.8 us (4%)
    pallas_call x1, Pallas kernels, attention(): pl.pallas_call(functools.partial(attention_kernel, n_sp, (DS, DL)), out_s...  139 us
    all_gather x1, waiting for transfers between devices, on_device(): down_whole = lax.all_gather(shrinking_matrix, 'sp', axis=1, tiled=True)  55.5 us
    reduce_scatter x1, waiting for transfers between devices, on_device(): lax.psum_scatter(partial_value.astype(jnp.bfloat16), 'tp', scatter_dimens...  36.6 us
    reduce_scatter x1, waiting for transfers between devices, on_device(): lax.psum_scatter(down_terms.astype(jnp.bfloat16), 'tp', scatter_dimension...  20 us
    all_gather x1, blocking collectives, on_device(): lax.all_gather(scaled.astype(jnp.bfloat16), 'tp', axis=1, tiled=True)  7.16 us
    dot_general x1, matrix products, on_device(): jnp.dot(activated, down_whole, preferred_element_type=jnp.float32)  7.06 us
    psum x1, blocking collectives, on_device(): square_total = lax.psum(jnp.sum(own_state * own_state, axis=1), 'tp')  6.06 us
  transfers between devices with their start and end apart: 3, of which 3 were waited for; matrix products, arithmetic and copies ran while one was open for 2% of the time, Pallas kernels for 0%

commit v1 on v0

v1 whole, which is shorter than its diff:
```python
import functools

import jax
import jax.numpy as jnp
from jax import lax
from jax.experimental import pallas as pl
from jax.experimental.pallas import tpu as pltpu
from jax.sharding import PartitionSpec as P

DS = 64
DL = 128
LANES = 128
MESH = pl.DeviceIdType.MESH

norm_epsilon = 1e-06
head_epsilon = 0.00064
key_epsilon = 1e-06


NN = (((1,), (0,)), ((), ()))
NT = (((1,), (1,)), ((), ()))


def split(x, count=2):
    if x.dtype == jnp.bfloat16:
        return [x]
    parts = []
    for _ in range(count - 1):
        high = x.astype(jnp.bfloat16)
        parts.append(high)
        x = x - high.astype(jnp.float32)
    return parts + [x.astype(jnp.bfloat16)]


def product(a, b, dims, count=2):
    total = None
    for i, p in enumerate(split(a, count)):
        for j, r in enumerate(split(b, count)):
            if i + j < count:
                term = lax.dot_general(p, r, dims, preferred_element_type=jnp.float32)
                total = term if total is None else total + term
    return total


def mm(a, b, count=2):
    return product(a, b, NN, count)


def mm_nt(a, b):
    return product(a, b, NT)


def sigmoid(x):
    return 1.0 / (1.0 + jnp.exp(-x))


def same_head(width):
    i = lax.broadcasted_iota(jnp.int32, (LANES, LANES), 0) // width
    j = lax.broadcasted_iota(jnp.int32, (LANES, LANES), 1) // width
    return (i == j).astype(jnp.float32).astype(jnp.bfloat16)


def unit_inverse(strict_part, rows, cols):
    size = strict_part.shape[0]
    inverse = (rows == cols).astype(jnp.float32)
    half = 1
    while half < size:
        off = (rows // (2 * half) == cols // (2 * half)) & (rows // half != cols // half)
        part = jnp.where(off, strict_part, 0.0)
        if half == 1:
            inverse = inverse + part
        else:
            inverse = inverse + mm(mm(inverse, part), inverse)
        half *= 2
    return inverse


def local_unit(width, q, k, v, fade, speed, extra):
    T = q.shape[0]
    ones = same_head(width)
    log_decay = extra - jnp.exp(jnp.float32(-0.5)) * sigmoid(fade)
    removal = k * lax.rsqrt(mm(k * k, ones) + key_epsilon)
    left = -removal
    right = sigmoid(speed) * removal
    rows = lax.broadcasted_iota(jnp.int32, (T, T), 0)
    cols = lax.broadcasted_iota(jnp.int32, (T, T), 1)
    inclusive = rows >= cols
    strict = rows > cols
    cumulative = mm(inclusive.astype(jnp.float32).astype(jnp.bfloat16), log_decay, 3)
    middle = cumulative[T // 2 : T // 2 + 1, :]
    final = cumulative[T - 1 : T, :]
    forward = jnp.exp(cumulative - middle)
    backward = jnp.exp(middle - cumulative)
    tail = jnp.exp(final - cumulative)
    queries = jnp.concatenate([left * jnp.exp(-log_decay) * forward, q * forward], axis=0)
    sources = jnp.concatenate([right * backward, k * backward], axis=0)
    start_target = left * jnp.exp(cumulative - log_decay)
    right_tail = right * tail
    key_tail = k * tail
    eye = lax.broadcasted_iota(jnp.int32, (LANES, LANES), 0) == lax.broadcasted_iota(
        jnp.int32, (LANES, LANES), 1
    )
    transit = jnp.where(eye, jnp.exp(final), 0.0)
    start_read = q * jnp.exp(cumulative)
    added = jnp.zeros((LANES, LANES), jnp.float32)
    local_out = jnp.zeros((T, LANES), jnp.float32)
    lane = lax.broadcasted_iota(jnp.int32, (1, LANES), 1) // width
    for head in range(LANES // width):
        only = lane == head
        pick = (lambda a: a) if width == LANES else (lambda a: jnp.where(only, a, 0.0))
        pairs = mm_nt(pick(queries), sources)
        remove_remove = jnp.where(strict, pairs[:T, :T], 0.0)
        remove_key = jnp.where(strict, pairs[:T, T:], 0.0)
        read_remove = jnp.where(inclusive, pairs[T:, :T], 0.0)
        read_key = jnp.where(inclusive, pairs[T:, T:], 0.0)
        inverse = unit_inverse(remove_remove, rows, cols)
        value = pick(v)
        carried = mm(inverse, mm(remove_key, value))
        start = mm(inverse, pick(start_target))
        local_out = local_out + mm(read_remove, carried) + mm(read_key, value)
        start_read = start_read + mm(read_remove, start)
        head_right = pick(right_tail)
        transit = transit + mm(start.T, head_right)
        added = added + mm(carried.T, head_right) + mm(value.T, pick(key_tail))
    return local_out, start_read, transit, added


def finish_unit(width, read, q, k, v, gain, own, gate):
    ones = same_head(width)
    mean = mm(read, ones) / width
    centered = read - mean
    variance = mm(centered * centered, ones) / width
    normed = centered * lax.rsqrt(variance + head_epsilon) * gain
    diagonal = mm(q * k * own, ones) * v
    return ((normed + diagonal) * gate).astype(jnp.bfloat16)


def members_of(n_sp):
    best = 1
    for count in range(1, n_sp + 1):
        if n_sp % count == 0 and count * count <= 2 * n_sp:
            best = count
    return best


def layer_kernel(
    n_sp, n_tp, widths, q_ref, k_ref, v_ref, f_ref, a_ref, e_ref, g_ref, gain_ref, own_ref,
    residual_ref, scale_ref, project_hbm, gate_hbm, up_hbm, down_hbm,
    out_ref,
    local_ref, read_ref, near, total_move, total_add, chain_in, chain_out, mixed_ref, project,
    wide, tall, term_send, term_got, hidden, active, summed,
    low_send, low_got, high_send, high_got, line_send, line_got,
    project_sem, keep_sem, out_sem, in_sem, pass_out, pass_in,
    near_out, near_in, chain_sem_out, chain_sem_in, term_out, term_in,
    row_out, row_in, up_out, up_in, side_out, side_in,
    low_out, low_in, high_out, high_in, line_out, line_in,
):
    F = members_of(n_sp)
    T = n_sp // F
    LO = 2 if n_tp % 2 == 0 else 1
    HI = n_tp // LO
    me = lax.axis_index("sp")
    t = lax.axis_index("tp")
    m, g = me // T, me % T
    hi, lo = t // LO, t % LO
    tokens = q_ref.shape[1]
    rows = gate_hbm.shape[0]
    depth = hidden.shape[1]
    own_cols = depth // n_tp
    down_cols = down_hbm.shape[1]
    base, extra = divmod(gate_hbm.shape[1] // LANES, F)
    parts = 2 if extra else 1

    def member(d):
        return lax.rem(m + d + F, F)

    def other(e):
        return lax.rem(g + e + T, T)

    def cell(h, l):
        return lax.rem(hi + h + HI, HI) * LO + lax.rem(lo + l + LO, LO)

    def remote(src, dst, send, recv, sp, tp):
        return pltpu.make_async_remote_copy(
            src_ref=src, dst_ref=dst, send_sem=send, recv_sem=recv,
            device_id=(sp, tp), device_id_type=MESH,
        )

    barrier = pltpu.get_barrier_semaphore()

    def greet(sp, tp):
        pl.semaphore_signal(barrier, inc=1, device_id=(sp, tp), device_id_type=MESH)

    for d in range(1, F):
        greet(member(d) * T + g, t)
    for e in range(1, T):
        greet(m * T + other(e), t)
    for d in range(1, n_tp):
        greet(me, lax.rem(t + d, n_tp))
    project_copy = pltpu.make_async_copy(project_hbm, project, project_sem)
    project_copy.start()
    pl.semaphore_wait(barrier, F + T + n_tp - 3)

    def source(w, part, dest):
        tile = dest * base + jnp.minimum(dest, extra) + (base if part else 0)
        at = pl.ds(pl.multiple_of(tile * LANES, LANES), LANES if part else base * LANES)
        return down_hbm.at[at, :] if w == 2 else (gate_hbm, up_hbm)[w].at[:, at]

    def landing(w, part, s):
        at = pl.ds(base * LANES if part else 0, LANES if part else base * LANES)
        if w == 2:
            return tall.at[s, at, :]
        return wide.at[w, pl.ds(pl.multiple_of(s * rows, rows), rows), at]

    def guarded(part, dest, action):
        if part:
            pl.when(dest < extra)(action)
        else:
            action()

    def give(w, part, d):
        dest = member(d)
        return remote(
            source(w, part, dest), landing(w, part, me), out_sem.at[w, part, d],
            in_sem.at[w, part, d], dest * T + g, t,
        )

    def take(w, part, d):
        return remote(
            source(w, part, m), landing(w, part, member(-d) * T + g), out_sem.at[w, part, d],
            in_sem.at[w, part, d], me, t,
        )

    def hand(w, part, d, e):
        s = member(-d) * T + g
        src = source(w, part, m) if d == 0 else landing(w, part, s)
        return remote(
            src, landing(w, part, s), pass_out.at[w, part, d, e], pass_in.at[w, part, d, e],
            m * T + other(e), t,
        )

    def accept(w, part, d, e):
        s = member(-d) * T + other(-e)
        return remote(
            source(w, part, m), landing(w, part, s), pass_out.at[w, part, d, e],
            pass_in.at[w, part, d, e], me, t,
        )

    def keep(w, part):
        return pltpu.make_async_copy(
            source(w, part, m), landing(w, part, me), keep_sem.at[w, part]
        )

    def open_weight(w):
        for part in range(parts):

            def begin():
                keep(w, part).start()
                for e in range(1, T):
                    hand(w, part, 0, e).start()

            guarded(part, m, begin)

    def send_weight(w, upward):
        for d in range(F - 1, 0, -1):
            for part in range(parts):
                dest = member(d)
                chosen = dest > m if upward else dest < m
                if part:
                    chosen = chosen & (dest < extra)
                pl.when(chosen)(lambda: give(w, part, d).start())

    def relay_weight(w):
        for d in range(1, F):
            for part in range(parts):

                def pass_on():
                    take(w, part, d).wait_recv()
                    for e in range(1, T):
                        hand(w, part, d, e).start()

                guarded(part, m, pass_on)

    def arrived_weight(w):
        for part in range(parts):

            def settle():
                keep(w, part).wait()
                for d in range(F):
                    for e in range(1, T):
                        accept(w, part, d, e).wait_recv()

            guarded(part, m, settle)

    open_weight(0)
    send_weight(0, True)
    send_weight(0, False)
    if extra:

        @pl.when(m >= extra)
        def _():
            tall[:, base * LANES :, :] = jnp.zeros(
                (n_sp, LANES, down_cols), jnp.bfloat16
            )

    per_group = q_ref.shape[2] // LANES

    def load(ref, group, c):
        return ref[group, :, c * LANES : (c + 1) * LANES].astype(jnp.float32)

    units = [(group, c) for group in range(2) for c in range(per_group)]

    def near_copy(u, e):
        return remote(
            near.at[g, u], near.at[g, u], near_out.at[u, e], near_in.at[u, e],
            m * T + other(e), t,
        )

    def near_take(u, e):
        return remote(
            near.at[other(-e), u], near.at[other(-e), u], near_out.at[u, e],
            near_in.at[u, e], me, t,
        )

    for u, (group, c) in enumerate(units):
        local_out, start_read, transit, added = local_unit(
            widths[group],
            *(load(r, group, c) for r in (q_ref, k_ref, v_ref, f_ref, a_ref, e_ref)),
        )
        local_ref[u] = local_out
        read_ref[u] = start_read
        near[g, u, 0] = transit.astype(jnp.bfloat16)
        near[g, u, 1] = added.astype(jnp.bfloat16)
    for u in range(len(units)):
        for e in range(1, T):
            near_copy(u, e).start()

    @pl.when(m == 0)
    def _():
        chain_in[...] = jnp.zeros_like(chain_in)

    send_weight(1, False)
    open_weight(1)
    relay_weight(0)

    def chain_copy(u):
        return remote(
            chain_out.at[u], chain_in.at[u], chain_sem_out.at[u], chain_sem_in.at[u],
            member(1) * T + g, t,
        )

    for u in range(len(units)):
        for e in range(1, T):
            near_take(u, e).wait_recv()
        move, add = near[0, u, 0], near[0, u, 1].astype(jnp.float32)
        for other_g in range(1, T):
            step = near[other_g, u, 0]
            add = mm(add, step) + near[other_g, u, 1].astype(jnp.float32)
            move = mm(move, step).astype(jnp.bfloat16)
        total_move[u] = move
        total_add[u] = add
    for u in range(len(units)):

        @pl.when(m > 0)
        def _():
            chain_copy(u).wait_recv()

        following = mm(chain_in[u], total_move[u]) + total_add[u]
        chain_out[u] = following.astype(jnp.bfloat16)

        @pl.when(m < F - 1)
        def _():
            chain_copy(u).start()

    send_weight(1, True)

    def fold(other_g, states):
        return tuple(
            mm(s, near[other_g, u, 0]) + near[other_g, u, 1].astype(jnp.float32)
            for u, s in enumerate(states)
        )

    states = lax.fori_loop(
        0, g, fold, tuple(chain_in[u].astype(jnp.float32) for u in range(len(units)))
    )
    for u, (group, c) in enumerate(units):
        lanes = slice(c * LANES, (c + 1) * LANES)
        read = local_ref[u] + mm_nt(read_ref[u], states[u])
        mixed_ref[:, u * LANES : (u + 1) * LANES] = finish_unit(
            widths[group], read, load(q_ref, group, c), load(k_ref, group, c),
            load(v_ref, group, c), gain_ref[group : group + 1, lanes],
            own_ref[group : group + 1, lanes], load(g_ref, group, c),
        )

    project_copy.wait()
    mixed = mixed_ref[...]

    def columns(at):
        return pl.ds(pl.multiple_of(at * own_cols, own_cols), own_cols)

    def term(at):
        return jnp.dot(mixed, project[:, columns(at)], preferred_element_type=jnp.float32)

    def term_copy(d):
        return remote(
            term_send.at[d], term_got.at[d], term_out.at[d], term_in.at[d],
            me, lax.rem(t + d, n_tp),
        )

    for d in range(1, n_tp):
        term_send[d] = term(lax.rem(t + d, n_tp)).astype(jnp.bfloat16)
        term_copy(d).start()
    branch = term(t).astype(jnp.bfloat16).astype(jnp.float32)
    open_weight(2)
    send_weight(2, True)
    send_weight(2, False)
    relay_weight(1)
    for d in range(1, n_tp):
        term_copy(d).wait_recv()
        branch = branch + term_got[d].astype(jnp.float32)

    def positions(at):
        return pl.ds(pl.multiple_of(at * tokens, tokens), tokens)

    own_state = (residual_ref[:, columns(t)].astype(jnp.float32) + branch).astype(jnp.bfloat16)
    hidden[positions(m), columns(t)] = own_state

    def row_copy(d):
        block = hidden.at[positions(m), columns(t)]
        return remote(block, block, row_out.at[d], row_in.at[d], member(d) * T + g, t)

    def row_take(d):
        block = hidden.at[positions(member(-d)), columns(t)]
        return remote(block, block, row_out.at[d], row_in.at[d], me, t)

    def up_copy(d, h):
        block = hidden.at[positions(member(-d)), columns(t)]
        return remote(block, block, up_out.at[d, h], up_in.at[d, h], me, cell(h, 0))

    def up_take(d, h):
        block = hidden.at[positions(member(-d)), columns(cell(-h, 0))]
        return remote(block, block, up_out.at[d, h], up_in.at[d, h], me, t)

    def side_copy(d, h, l):
        block = hidden.at[positions(member(-d)), columns(cell(-h, 0))]
        return remote(block, block, side_out.at[d, h, l], side_in.at[d, h, l], me, cell(0, l))

    def side_take(d, h, l):
        block = hidden.at[positions(member(-d)), columns(cell(-h, -l))]
        return remote(block, block, side_out.at[d, h, l], side_in.at[d, h, l], me, t)

    for d in range(F - 1, 0, -1):
        row_copy(d).start()
    for d in range(F + 1):
        if d < F:
            if d:
                row_take(d).wait_recv()
            for h in range(1, HI):
                up_copy(d, h).start()
            for l in range(1, LO):
                side_copy(d, 0, l).start()
        if d:
            for h in range(1, HI):
                up_take(d - 1, h).wait_recv()
                for l in range(1, LO):
                    side_copy(d - 1, h, l).start()
    for d in range(F):
        for h in range(HI):
            for l in range(1, LO):
                side_take(d, h, l).wait_recv()

    arrived_weight(0)
    arrived_weight(1)
    width = wide.shape[2]
    have = (base + (m < extra).astype(jnp.int32)) * LANES if extra else width

    @pl.loop(0, F)
    def _(i):
        state = hidden[positions(i), :].astype(jnp.float32)
        power = jnp.sum(state * state, axis=1, keepdims=True) / depth
        normed = (state * lax.rsqrt(power + norm_epsilon) * scale_ref[...]).astype(jnp.bfloat16)
        gate_pre = jnp.dot(normed, wide[0], preferred_element_type=jnp.float32)
        up_pre = jnp.dot(normed, wide[1], preferred_element_type=jnp.float32)
        value = gate_pre / (1.0 + jnp.exp(-gate_pre)) * up_pre
        if extra:
            lane = lax.broadcasted_iota(jnp.int32, (1, width), 1)
            value = jnp.where(lane < have, value, 0.0)
        active[positions(i), :] = value.astype(jnp.bfloat16)

    relay_weight(2)
    arrived_weight(2)

    @pl.loop(0, F)
    def _(i):
        block = active[positions(i), :]
        for s in range(n_sp):
            summed[positions(i), s * down_cols : (s + 1) * down_cols] = jnp.dot(
                block, tall[s], preferred_element_type=jnp.float32
            )

    def low_copy(d, h, l):
        return remote(
            low_send.at[d, h, l], low_got.at[d, h, l], low_out.at[d, h, l],
            low_in.at[d, h, l], me, cell(0, l),
        )

    def high_copy(d, h):
        return remote(
            high_send.at[d, h], high_got.at[d, h], high_out.at[d, h], high_in.at[d, h],
            me, cell(h, 0),
        )

    def line_copy(d):
        return remote(
            line_send.at[d], line_got.at[d], line_out.at[d], line_in.at[d], member(d) * T + g, t
        )

    order = list(range(F - 1, 0, -1)) + [0]
    for d in order:
        for h in range(HI):
            for l in range(1, LO):
                low_send[d, h, l] = summed[positions(member(d)), columns(cell(h, l))].astype(
                    jnp.bfloat16
                )
                low_copy(d, h, l).start()

    def two_cores(d, h):
        value = summed[positions(member(d)), columns(cell(h, 0))]
        for l in range(1, LO):
            value = value + low_got[d, h, l].astype(jnp.float32)
        return value

    for d in order:
        for h in range(HI):
            for l in range(1, LO):
                low_copy(d, h, l).wait_recv()
        for h in range(1, HI):
            high_send[d, h] = two_cores(d, h).astype(jnp.bfloat16)
            high_copy(d, h).start()

    for d in order:
        value = two_cores(d, 0)
        for h in range(1, HI):
            high_copy(d, h).wait_recv()
            value = value + high_got[d, h].astype(jnp.float32)
        if d:
            line_send[d] = value.astype(jnp.bfloat16)
            line_copy(d).start()
    for d in range(1, F):
        line_copy(d).wait_recv()
        value = value + line_got[d].astype(jnp.float32)
    out_ref[...] = (
        hidden[positions(m), columns(t)].astype(jnp.float32) + value
    ).astype(jnp.bfloat16)

    for w in range(3):
        for part in range(parts):
            for d in range(1, F):
                guarded(part, member(d), lambda: give(w, part, d).wait_send())

            def passed():
                for d in range(F):
                    for e in range(1, T):
                        hand(w, part, d, e).wait_send()

            guarded(part, m, passed)
    for u in range(len(units)):
        for e in range(1, T):
            near_copy(u, e).wait_send()

    @pl.when(m < F - 1)
    def _():
        for u in range(len(units)):
            chain_copy(u).wait_send()

    for d in range(1, n_tp):
        term_copy(d).wait_send()
    for d in range(F):
        if d:
            row_copy(d).wait_send()
            line_copy(d).wait_send()
        for h in range(HI):
            if h:
                up_copy(d, h).wait_send()
                high_copy(d, h).wait_send()
            for l in range(1, LO):
                side_copy(d, h, l).wait_send()
                low_copy(d, h, l).wait_send()


def layer(n_sp, n_tp, q, k, v, f, a, e, g, gain, own, residual, scale, project, gate, up, down):
    tokens, channels = q.shape[1], q.shape[2]
    units = 2 * channels // LANES
    depth = residual.shape[1]
    cols = depth // n_tp
    F = members_of(n_sp)
    T = n_sp // F
    LO = 2 if n_tp % 2 == 0 else 1
    HI = n_tp // LO
    width = -(-(gate.shape[1] // LANES) // F) * LANES
    vmem = pl.BlockSpec(memory_space=pltpu.VMEM)
    hbm = pl.BlockSpec(memory_space=pl.ANY)
    bf16, f32 = jnp.bfloat16, jnp.float32
    sem = pltpu.SemaphoreType.DMA
    scratch = [
        pltpu.VMEM((units, tokens, LANES), f32),
        pltpu.VMEM((units, tokens, LANES), f32),
        pltpu.VMEM((T, units, 2, LANES, LANES), bf16),
        pltpu.VMEM((units, LANES, LANES), bf16),
        pltpu.VMEM((units, LANES, LANES), f32),
        pltpu.VMEM((units, LANES, LANES), bf16),
        pltpu.VMEM((units, LANES, LANES), bf16),
        pltpu.VMEM((tokens, units * LANES), bf16),
        pltpu.VMEM(project.shape, bf16),
        pltpu.VMEM((2, depth, width), bf16),
        pltpu.VMEM((n_sp, width, down.shape[1]), bf16),
        pltpu.VMEM((n_tp, tokens, cols), bf16),
        pltpu.VMEM((n_tp, tokens, cols), bf16),
        pltpu.VMEM((F * tokens, depth), bf16),
        pltpu.VMEM((F * tokens, width), bf16),
        pltpu.VMEM((F * tokens, depth), f32),
        pltpu.VMEM((F, HI, LO, tokens, cols), bf16),
        pltpu.VMEM((F, HI, LO, tokens, cols), bf16),
        pltpu.VMEM((F, HI, tokens, cols), bf16),
        pltpu.VMEM((F, HI, tokens, cols), bf16),
        pltpu.VMEM((F, tokens, cols), bf16),
        pltpu.VMEM((F, tokens, cols), bf16),
        sem, sem((3, 2)),
    ]
    for shape in (
        (3, 2, F), (3, 2, F, T), (units, T), (units,), (n_tp,), (F,), (F, HI), (F, HI, LO),
        (F, HI, LO), (F, HI), (F,),
    ):
        scratch += [sem(shape), sem(shape)]
    return pl.pallas_call(
        functools.partial(layer_kernel, n_sp, n_tp, (DS, DL)),
        out_shape=jax.ShapeDtypeStruct((tokens, cols), bf16),
        in_specs=[vmem] * 11 + [hbm] * 4,
        out_specs=vmem,
        scratch_shapes=scratch,
        compiler_params=pltpu.CompilerParams(
            collective_id=0, has_side_effects=True, vmem_limit_bytes=60 * 2**20
        ),
        name="layer",
    )(q, k, v, f, a, e, g, gain, own, residual, scale, project, gate, up, down)


def on_device(
    stratum_source_matrix,
    acceptance_query,
    cluster_lookup_matrix,
    cluster_payload_matrix,
    fading_logit,
    adaptation_speed_logit,
    additional_fading_exponent,
    result_switch_pair,
    attender_scaling_factor,
    present_item_factor,
    final_mapping_matrix,
    perceptron_scaling_factor,
    switching_matrix,
    widening_matrix,
    shrinking_matrix,
):
    return layer(
        lax.axis_size("sp"),
        lax.axis_size("tp"),
        acceptance_query,
        cluster_lookup_matrix,
        cluster_payload_matrix,
        fading_logit,
        adaptation_speed_logit,
        additional_fading_exponent,
        result_switch_pair,
        attender_scaling_factor,
        present_item_factor,
        stratum_source_matrix,
        perceptron_scaling_factor.reshape(1, -1),
        final_mapping_matrix.reshape(-1, final_mapping_matrix.shape[2]),
        switching_matrix,
        widening_matrix,
        shrinking_matrix,
    )


def solution(mesh):
    tokens = P(None, "sp", "tp")
    in_specs = (
        P("sp", None), tokens, tokens, tokens, tokens, tokens, tokens, tokens,
        P(None, "tp"), P(None, "tp"), P(None, "tp", None), P(),
        P("sp", "tp"), P("sp", "tp"), P("tp", "sp"),
    )
    return jax.shard_map(
        on_device, mesh=mesh, in_specs=in_specs, out_specs=P("sp", "tp"), check_vma=False
    )
```

time: 296 us -> 124 us (0.42)
  waiting for transfers between devices: 113 us -> 0 us
  Pallas kernels: 139 us -> 122 us
  between operations: 14.9 us -> 0.01 us
  blocking collectives: 13.2 us -> 0 us
  matrix products: 12.8 us -> 0 us
    reduce_scatter x2 -> x0, waiting for transfers between devices: 56.6 us -> none  [the longest x1 36.6 us: on_device(): lax.psum_scatter(partial_value.astype(jnp.bfloat16), 'tp', scatter_dimens...]
    all_gather x1 -> x0, waiting for transfers between devices: 55.5 us -> none  [on_device(): down_whole = lax.all_gather(shrinking_matrix, 'sp', axis=1, tiled=True)]
    pallas_call x1, Pallas kernels: 139 us -> 122 us  [layer(): pl.pallas_call(functools.partial(layer_kernel, n_sp, n_tp, (DS, DL)), out...]
    dot_general x3 -> x0, matrix products: 12.8 us -> none  [the longest x1 7.06 us: on_device(): jnp.dot(activated, down_whole, preferred_element_type=jnp.float32)]
    all_gather x1 -> x0, blocking collectives: 7.16 us -> none  [on_device(): lax.all_gather(scaled.astype(jnp.bfloat16), 'tp', axis=1, tiled=True)]
    psum x1 -> x0, blocking collectives: 6.06 us -> none  [on_device(): square_total = lax.psum(jnp.sum(own_state * own_state, axis=1), 'tp')]
  transfers between devices with their start and end apart: 3 -> 0, of which waited for: 3 -> 0; matrix products, arithmetic and copies ran while one was open for 2% -> 0% of each run, Pallas kernels for 0% -> 0%
where the time goes in v1:
time: 124 us
  Pallas kernels  122 us (98%)
  local copies, waits for them, and re-layouts  1.57 us (1%)
    pallas_call x1, Pallas kernels, layer(): pl.pallas_call(functools.partial(layer_kernel, n_sp, n_tp, (DS, DL)), out...  122 us

profile of v1, /device:TPU:0, one launch (start us, length us, event | category | flops | bytes accessed | tf_op | source)
XLA Modules:
  0.0 123.6 jit_solution(12062593199512979658)
XLA Ops:
  0.0 122.0 %layer.1 = bf16[128,512]{1,0:T(8,128)(2,1)} custom-call(bf16[2,128,256]{2,1,0:T(8,128)(2,1)} %q_ref.1, bf16[2,128,256]{2,1,0:T(8,128)(2,1)} %k_ref.1, bf16[2,128,256]{2,1,0:T(8,128)(2,1)} %v_ref.1, bf16[2,128,256]{2,1,0:T(8,128)(2,1)} %f_ref.1, bf16[2,128,256]{2,1,0:T(8,128)(2,1)} %a_ref.1, f32[2,128,256]{2,1,0:T(8,128)} %e_ref.1, ...), custom_call_target="tpu_custom_call" | custom-call | tf_op jit(solution)/shard_map/layer/pallas_call | solution.py:635
  122.0 1.6 %copy.17 = bf16[128,512]{1,0:T(8,128)(2,1)} copy(bf16[128,512]{1,0:T(8,128)(2,1)} %layer.1) | data formatting | bytes 262144

commit v2 on v1

--- a/solution.py
+++ b/solution.py
@@ -148,10 +148,10 @@
     residual_ref, scale_ref, project_hbm, gate_hbm, up_hbm, down_hbm,
     out_ref,
     local_ref, read_ref, near, total_move, total_add, chain_in, chain_out, mixed_ref, project,
-    wide, tall, term_send, term_got, hidden, active, summed,
+    wide, tall, pair_send, pair_got, term_send, term_got, hidden, active, summed,
     low_send, low_got, high_send, high_got, line_send, line_got,
     project_sem, keep_sem, out_sem, in_sem, pass_out, pass_in,
-    near_out, near_in, chain_sem_out, chain_sem_in, term_out, term_in,
+    near_out, near_in, chain_sem_out, chain_sem_in, pair_out, pair_in, term_out, term_in,
     row_out, row_in, up_out, up_in, side_out, side_in,
     low_out, low_in, high_out, high_in, line_out, line_in,
 ):
@@ -201,8 +201,12 @@
     project_copy.start()
     pl.semaphore_wait(barrier, F + T + n_tp - 3)
 
+    def more(dest):
+        return jnp.where(t % 2 == 0, dest < extra, dest >= F - extra)
+
     def source(w, part, dest):
-        tile = dest * base + jnp.minimum(dest, extra) + (base if part else 0)
+        before = jnp.where(t % 2 == 0, jnp.minimum(dest, extra), jnp.maximum(dest - F + extra, 0))
+        tile = dest * base + before + (base if part else 0)
         at = pl.ds(pl.multiple_of(tile * LANES, LANES), LANES if part else base * LANES)
         return down_hbm.at[at, :] if w == 2 else (gate_hbm, up_hbm)[w].at[:, at]
 
@@ -214,7 +218,7 @@
 
     def guarded(part, dest, action):
         if part:
-            pl.when(dest < extra)(action)
+            pl.when(more(dest))(action)
         else:
             action()
 
@@ -261,18 +265,19 @@
 
             guarded(part, m, begin)
 
-    def send_weight(w, upward):
-        for d in range(F - 1, 0, -1):
-            for part in range(parts):
-                dest = member(d)
-                chosen = dest > m if upward else dest < m
-                if part:
-                    chosen = chosen & (dest < extra)
-                pl.when(chosen)(lambda: give(w, part, d).start())
-
-    def relay_weight(w):
-        for d in range(1, F):
-            for part in range(parts):
+    def send_weight(w, chosen_parts):
+        for part in chosen_parts:
+            for upward, ways in ((True, range(F - 1, 0, -1)), (False, range(1, F))):
+                for d in ways:
+                    dest = member(d)
+                    chosen = dest > m if upward else dest < m
+                    if part:
+                        chosen = chosen & more(dest)
+                    pl.when(chosen)(lambda: give(w, part, d).start())
+
+    def relay_weight(w, chosen_parts):
+        for part in chosen_parts:
+            for d in range(1, F):
 
                 def pass_on():
                     take(w, part, d).wait_recv()
@@ -292,12 +297,12 @@
 
             guarded(part, m, settle)
 
-    open_weight(0)
-    send_weight(0, True)
-    send_weight(0, False)
+    for w in range(2):
+        open_weight(w)
+        send_weight(w, range(parts))
     if extra:
 
-        @pl.when(m >= extra)
+        @pl.when(jnp.logical_not(more(m)))
         def _():
             tall[:, base * LANES :, :] = jnp.zeros(
                 (n_sp, LANES, down_cols), jnp.bfloat16
@@ -339,9 +344,7 @@
     def _():
         chain_in[...] = jnp.zeros_like(chain_in)
 
-    send_weight(1, False)
-    open_weight(1)
-    relay_weight(0)
+    relay_weight(0, range(parts))
 
     def chain_copy(u):
         return remote(
@@ -372,8 +375,6 @@
         def _():
             chain_copy(u).start()
 
-    send_weight(1, True)
-
     def fold(other_g, states):
         return tuple(
             mm(s, near[other_g, u, 0]) + near[other_g, u, 1].astype(jnp.float32)
@@ -401,23 +402,34 @@
     def term(at):
         return jnp.dot(mixed, project[:, columns(at)], preferred_element_type=jnp.float32)
 
-    def term_copy(d):
-        return remote(
-            term_send.at[d], term_got.at[d], term_out.at[d], term_in.at[d],
-            me, lax.rem(t + d, n_tp),
-        )
-
-    for d in range(1, n_tp):
-        term_send[d] = term(lax.rem(t + d, n_tp)).astype(jnp.bfloat16)
-        term_copy(d).start()
-    branch = term(t).astype(jnp.bfloat16).astype(jnp.float32)
-    open_weight(2)
-    send_weight(2, True)
-    send_weight(2, False)
-    relay_weight(1)
-    for d in range(1, n_tp):
-        term_copy(d).wait_recv()
-        branch = branch + term_got[d].astype(jnp.float32)
+    def pair_copy(h, l):
+        return remote(
+            pair_send.at[h, l], pair_got.at[h, l], pair_out.at[h, l], pair_in.at[h, l],
+            me, cell(0, l),
+        )
+
+    def term_copy(h):
+        return remote(
+            term_send.at[h], term_got.at[h], term_out.at[h], term_in.at[h], me, cell(h, 0)
+        )
+
+    far = list(range(1, HI)) + [0]
+    for h in far:
+        for l in range(1, LO):
+            pair_send[h, l] = term(cell(h, l)).astype(jnp.bfloat16)
+            pair_copy(h, l).start()
+    for h in far:
+        branch = term(cell(h, 0))
+        for l in range(1, LO):
+            pair_copy(h, l).wait_recv()
+            branch = branch + pair_got[h, l].astype(jnp.float32)
+        if h:
+            term_send[h] = branch.astype(jnp.bfloat16)
+            term_copy(h).start()
+    relay_weight(1, range(parts))
+    for h in range(1, HI):
+        term_copy(h).wait_recv()
+        branch = branch + term_got[h].astype(jnp.float32)
 
     def positions(at):
         return pl.ds(pl.multiple_of(at * tokens, tokens), tokens)
@@ -425,58 +437,40 @@
     own_state = (residual_ref[:, columns(t)].astype(jnp.float32) + branch).astype(jnp.bfloat16)
     hidden[positions(m), columns(t)] = own_state
 
-    def row_copy(d):
-        block = hidden.at[positions(m), columns(t)]
-        return remote(block, block, row_out.at[d], row_in.at[d], member(d) * T + g, t)
-
-    def row_take(d):
-        block = hidden.at[positions(member(-d)), columns(t)]
-        return remote(block, block, row_out.at[d], row_in.at[d], me, t)
-
-    def up_copy(d, h):
-        block = hidden.at[positions(member(-d)), columns(t)]
-        return remote(block, block, up_out.at[d, h], up_in.at[d, h], me, cell(h, 0))
-
-    def up_take(d, h):
-        block = hidden.at[positions(member(-d)), columns(cell(-h, 0))]
-        return remote(block, block, up_out.at[d, h], up_in.at[d, h], me, t)
-
-    def side_copy(d, h, l):
-        block = hidden.at[positions(member(-d)), columns(cell(-h, 0))]
-        return remote(block, block, side_out.at[d, h, l], side_in.at[d, h, l], me, cell(0, l))
-
-    def side_take(d, h, l):
-        block = hidden.at[positions(member(-d)), columns(cell(-h, -l))]
-        return remote(block, block, side_out.at[d, h, l], side_in.at[d, h, l], me, t)
-
-    for d in range(F - 1, 0, -1):
-        row_copy(d).start()
-    for d in range(F + 1):
-        if d < F:
-            if d:
-                row_take(d).wait_recv()
-            for h in range(1, HI):
-                up_copy(d, h).start()
-            for l in range(1, LO):
-                side_copy(d, 0, l).start()
-        if d:
-            for h in range(1, HI):
-                up_take(d - 1, h).wait_recv()
-                for l in range(1, LO):
-                    side_copy(d - 1, h, l).start()
-    for d in range(F):
-        for h in range(HI):
-            for l in range(1, LO):
-                side_take(d, h, l).wait_recv()
-
-    arrived_weight(0)
-    arrived_weight(1)
+    def block(a, at):
+        return hidden.at[positions(a), columns(at)]
+
+    def row_copy(a, d):
+        return remote(
+            block(a, t), block(a, t), row_out.at[d], row_in.at[a], member(d) * T + g, t
+        )
+
+    def up_copy(a, h):
+        return remote(block(a, t), block(a, t), up_out.at[a, h], up_in.at[a, h], me, cell(h, 0))
+
+    def up_take(a, h):
+        at = block(a, cell(-h, 0))
+        return remote(at, at, up_out.at[a, h], up_in.at[a, h], me, t)
+
+    def side_copy(a, h, l):
+        at = block(a, cell(-h, 0))
+        return remote(at, at, side_out.at[a, h, l], side_in.at[a, h, l], me, cell(0, l))
+
+    def side_take(a, h, l):
+        at = block(a, cell(-h, -l))
+        return remote(at, at, side_out.at[a, h, l], side_in.at[a, h, l], me, t)
+
+    def spread(a):
+        for h in range(1, HI):
+            up_copy(a, h).start()
+        for l in range(1, LO):
+            side_copy(a, 0, l).start()
+
     width = wide.shape[2]
-    have = (base + (m < extra).astype(jnp.int32)) * LANES if extra else width
-
-    @pl.loop(0, F)
-    def _(i):
-        state = hidden[positions(i), :].astype(jnp.float32)
+    have = (base + more(m).astype(jnp.int32)) * LANES if extra else width
+
+    def activate(a):
+        state = hidden[positions(a), :].astype(jnp.float32)
         power = jnp.sum(state * state, axis=1, keepdims=True) / depth
         normed = (state * lax.rsqrt(power + norm_epsilon) * scale_ref[...]).astype(jnp.bfloat16)
         gate_pre = jnp.dot(normed, wide[0], preferred_element_type=jnp.float32)
@@ -485,73 +479,117 @@
         if extra:
             lane = lax.broadcasted_iota(jnp.int32, (1, width), 1)
             value = jnp.where(lane < have, value, 0.0)
-        active[positions(i), :] = value.astype(jnp.bfloat16)
-
-    relay_weight(2)
+        active[positions(a), :] = value.astype(jnp.bfloat16)
+
+    for d in range(1, F):
+        pl.when(m + d < F)(lambda: row_copy(m, d).start())
+    for d in range(1, F):
+        pl.when(m + d >= F)(lambda: row_copy(m, d).start())
+    spread(m)
+    open_weight(2)
+    send_weight(2, range(parts))
+
+    @pl.loop(0, F + 2)
+    def _(i):
+        @pl.when((i < F) & (i != m))
+        def _():
+            row_copy(i, 0).wait_recv()
+            spread(i)
+
+        @pl.when((i >= 1) & (i <= F))
+        def _():
+            for h in range(1, HI):
+                up_take(i - 1, h).wait_recv()
+                for l in range(1, LO):
+                    side_copy(i - 1, h, l).start()
+
+        @pl.when(i == 2)
+        def _():
+            arrived_weight(0)
+            arrived_weight(1)
+
+        @pl.when(i >= 2)
+        def _():
+            for h in range(HI):
+                for l in range(1, LO):
+                    side_take(i - 2, h, l).wait_recv()
+            activate(i - 2)
+
+    relay_weight(2, range(parts))
     arrived_weight(2)
 
-    @pl.loop(0, F)
-    def _(i):
-        block = active[positions(i), :]
+    def target(k):
+        if k == F - 1:
+            return m
+        rising = k + (k >= m).astype(jnp.int32)
+        falling = F - 1 - k - (F - 1 - k <= m).astype(jnp.int32)
+        return jnp.where(2 * m >= F, rising, falling)
+
+    def low_copy(k, h, l):
+        return remote(
+            low_send.at[k, h, l], low_got.at[k, h, l], low_out.at[k, h, l],
+            low_in.at[k, h, l], me, cell(0, l),
+        )
+
+    def high_copy(k, h):
+        return remote(
+            high_send.at[k, h], high_got.at[k, h], high_out.at[k, h], high_in.at[k, h],
+            me, cell(h, 0),
+        )
+
+    def line_copy(k):
+        return remote(
+            line_send.at[k], line_got.at[m], line_out.at[k], line_in.at[m],
+            target(k) * T + g, t,
+        )
+
+    def line_take(a):
+        return remote(line_send.at[0], line_got.at[a], line_out.at[0], line_in.at[a], me, t)
+
+    for k in range(F):
+        here = positions(target(k))
+        units_here = active[here, :]
         for s in range(n_sp):
-            summed[positions(i), s * down_cols : (s + 1) * down_cols] = jnp.dot(
-                block, tall[s], preferred_element_type=jnp.float32
+            summed[here, s * down_cols : (s + 1) * down_cols] = jnp.dot(
+                units_here, tall[s], preferred_element_type=jnp.float32
             )
-
-    def low_copy(d, h, l):
-        return remote(
-            low_send.at[d, h, l], low_got.at[d, h, l], low_out.at[d, h, l],
-            low_in.at[d, h, l], me, cell(0, l),
-        )
-
-    def high_copy(d, h):
-        return remote(
-            high_send.at[d, h], high_got.at[d, h], high_out.at[d, h], high_in.at[d, h],
-            me, cell(h, 0),
-        )
-
-    def line_copy(d):
-        return remote(
-            line_send.at[d], line_got.at[d], line_out.at[d], line_in.at[d], member(d) * T + g, t
-        )
-
-    order = list(range(F - 1, 0, -1)) + [0]
-    for d in order:
+        for h in far:
+            for l in range(1, LO):
+                low_send[k, h, l] = summed[here, columns(cell(h, l))].astype(jnp.bfloat16)
+                low_copy(k, h, l).start()
+
+    def two_cores(k, h):
+        value = summed[positions(target(k)), columns(cell(h, 0))]
+        for l in range(1, LO):
+            value = value + low_got[k, h, l].astype(jnp.float32)
+        return value
+
+    for k in range(F):
         for h in range(HI):
             for l in range(1, LO):
-                low_send[d, h, l] = summed[positions(member(d)), columns(cell(h, l))].astype(
-                    jnp.bfloat16
-                )
-                low_copy(d, h, l).start()
-
-    def two_cores(d, h):
-        value = summed[positions(member(d)), columns(cell(h, 0))]
-        for l in range(1, LO):
-            value = value + low_got[d, h, l].astype(jnp.float32)
-        return value
-
-    for d in order:
-        for h in range(HI):
-            for l in range(1, LO):
-                low_copy(d, h, l).wait_recv()
+                low_copy(k, h, l).wait_recv()
         for h in range(1, HI):
-            high_send[d, h] = two_cores(d, h).astype(jnp.bfloat16)
-            high_copy(d, h).start()
-
-    for d in order:
-        value = two_cores(d, 0)
+            high_send[k, h] = two_cores(k, h).astype(jnp.bfloat16)
+            high_copy(k, h).start()
+
+    for k in range(F):
+        value = two_cores(k, 0)
         for h in range(1, HI):
-            high_copy(d, h).wait_recv()
-            value = value + high_got[d, h].astype(jnp.float32)
-        if d:
-            line_send[d] = value.astype(jnp.bfloat16)
-            line_copy(d).start()
-    for d in range(1, F):
-        line_copy(d).wait_recv()
-        value = value + line_got[d].astype(jnp.float32)
-    out_ref[...] = (
-        hidden[positions(m), columns(t)].astype(jnp.float32) + value
-    ).astype(jnp.bfloat16)
+            high_copy(k, h).wait_recv()
+            value = value + high_got[k, h].astype(jnp.float32)
+        if k < F - 1:
+            line_send[k] = value.astype(jnp.bfloat16)
+            line_copy(k).start()
+    summed[:tokens, :own_cols] = hidden[positions(m), columns(t)].astype(jnp.float32) + value
+
+    @pl.loop(0, F)
+    def _(a):
+        @pl.when(a != m)
+        def _():
+            line_take(a).wait_recv()
+            summed[:tokens, :own_cols] += line_got[a].astype(jnp.float32)
+
+    out_ref[...] = summed[:tokens, :own_cols].astype(jnp.bfloat16)
 
     for w in range(3):
         for part in range(parts):
@@ -573,12 +611,15 @@
         for u in range(len(units)):
             chain_copy(u).wait_send()
 
-    for d in range(1, n_tp):
-        term_copy(d).wait_send()
+    for h in range(HI):
+        if h:
+            term_copy(h).wait_send()
+        for l in range(1, LO):
+            pair_copy(h, l).wait_send()
     for d in range(F):
         if d:
-            row_copy(d).wait_send()
-            line_copy(d).wait_send()
+            row_copy(m, d).wait_send()
+            line_copy(d - 1).wait_send()
         for h in range(HI):
             if h:
                 up_copy(d, h).wait_send()
@@ -614,8 +655,10 @@
         pltpu.VMEM(project.shape, bf16),
         pltpu.VMEM((2, depth, width), bf16),
         pltpu.VMEM((n_sp, width, down.shape[1]), bf16),
-        pltpu.VMEM((n_tp, tokens, cols), bf16),
-        pltpu.VMEM((n_tp, tokens, cols), bf16),
+        pltpu.VMEM((HI, LO, tokens, cols), bf16),
+        pltpu.VMEM((HI, LO, tokens, cols), bf16),
+        pltpu.VMEM((HI, tokens, cols), bf16),
+        pltpu.VMEM((HI, tokens, cols), bf16),
         pltpu.VMEM((F * tokens, depth), bf16),
         pltpu.VMEM((F * tokens, width), bf16),
         pltpu.VMEM((F * tokens, depth), f32),
@@ -628,7 +671,7 @@
         sem, sem((3, 2)),
     ]
     for shape in (
-        (3, 2, F), (3, 2, F, T), (units, T), (units,), (n_tp,), (F,), (F, HI), (F, HI, LO),
+        (3, 2, F), (3, 2, F, T), (units, T), (units,), (HI, LO), (HI,), (F,), (F, HI), (F, HI, LO),
         (F, HI, LO), (F, HI), (F,),
     ):
         scratch += [sem(shape), sem(shape)]

time: 124 us -> 109 us (0.88)
  Pallas kernels: 122 us -> 108 us
    pallas_call x1, Pallas kernels: 122 us -> 108 us  [layer(): pl.pallas_call(functools.partial(layer_kernel, n_sp, n_tp, (DS, DL)), out...]
where the time goes in v2:
time: 109 us
  Pallas kernels  108 us (99%)
  local copies, waits for them, and re-layouts  1.57 us (1%)
    pallas_call x1, Pallas kernels, layer(): pl.pallas_call(functools.partial(layer_kernel, n_sp, n_tp, (DS, DL)), out...  108 us

profile of v2, /device:TPU:0, one launch (start us, length us, event | category | flops | bytes accessed | tf_op | source)
XLA Modules:
  0.0 109.3 jit_solution(3608406632763320606)
XLA Ops:
  0.0 107.7 %layer.1 = bf16[128,512]{1,0:T(8,128)(2,1)} custom-call(bf16[2,128,256]{2,1,0:T(8,128)(2,1)} %q_ref.1, bf16[2,128,256]{2,1,0:T(8,128)(2,1)} %k_ref.1, bf16[2,128,256]{2,1,0:T(8,128)(2,1)} %v_ref.1, bf16[2,128,256]{2,1,0:T(8,128)(2,1)} %f_ref.1, bf16[2,128,256]{2,1,0:T(8,128)(2,1)} %a_ref.1, f32[2,128,256]{2,1,0:T(8,128)} %e_ref.1, ...), custom_call_target="tpu_custom_call" | custom-call | tf_op jit(solution)/shard_map/layer/pallas_call | solution.py:678
  107.7 1.6 %copy.17 = bf16[128,512]{1,0:T(8,128)(2,1)} copy(bf16[128,512]{1,0:T(8,128)(2,1)} %layer.1) | data formatting | bytes 262144

commit v3 on v2

--- a/solution.py
+++ b/solution.py
@@ -19,6 +19,7 @@
 
 NN = (((1,), (0,)), ((), ()))
 NT = (((1,), (1,)), ((), ()))
+TN = (((0,), (0,)), ((), ()))
 
 
 def split(x, count=2):
@@ -60,69 +61,113 @@
     return (i == j).astype(jnp.float32).astype(jnp.bfloat16)
 
 
-def unit_inverse(strict_part, rows, cols):
-    size = strict_part.shape[0]
-    inverse = (rows == cols).astype(jnp.float32)
+def pair_up(a, b):
+    zero = jnp.zeros_like(a)
+    return jnp.concatenate(
+        [jnp.concatenate([a, zero], axis=1), jnp.concatenate([zero, b], axis=1)], axis=0
+    )
+
+
+def unit_inverses(strict_parts, rows, cols):
+    size = strict_parts[0].shape[0]
+    pairs = [strict_parts[i : i + 2] for i in range(0, len(strict_parts), 2)]
+    eye = (rows == cols).astype(jnp.float32)
+    inverses = None
     half = 1
     while half < size:
         off = (rows // (2 * half) == cols // (2 * half)) & (rows // half != cols // half)
-        part = jnp.where(off, strict_part, 0.0)
+        parts = [[jnp.where(off, s, 0.0) for s in pair] for pair in pairs]
         if half == 1:
-            inverse = inverse + part
+            inverses = [jnp.concatenate([eye + p for p in pair], axis=1) for pair in parts]
         else:
-            inverse = inverse + mm(mm(inverse, part), inverse)
+            middles = [
+                product_of(split(inverse), [pair_up(*x) for x in zip(*(split(p) for p in pair))])
+                for inverse, pair in zip(inverses, parts)
+            ]
+            inverses = [
+                inverse
+                + product_of(
+                    split(middle),
+                    [pair_up(x[:, :size], x[:, size:]) for x in split(inverse)],
+                )
+                for inverse, middle in zip(inverses, middles)
+            ]
         half *= 2
-    return inverse
-
-
-def local_unit(width, q, k, v, fade, speed, extra):
-    T = q.shape[0]
-    ones = same_head(width)
-    log_decay = extra - jnp.exp(jnp.float32(-0.5)) * sigmoid(fade)
-    removal = k * lax.rsqrt(mm(k * k, ones) + key_epsilon)
-    left = -removal
-    right = sigmoid(speed) * removal
+    return [inverse[:, i * size : (i + 1) * size] for inverse in inverses for i in range(2)]
+
+
+def product_of(left, right, dims=NN):
+    total = None
+    for i, p in enumerate(left):
+        for j, r in enumerate(right):
+            if i + j < 2:
+                term = lax.dot_general(p, r, dims, preferred_element_type=jnp.float32)
+                total = term if total is None else total + term
+    return total
+
+
+def local_units(widths, tokens):
+    T = tokens[0][0].shape[0]
     rows = lax.broadcasted_iota(jnp.int32, (T, T), 0)
     cols = lax.broadcasted_iota(jnp.int32, (T, T), 1)
     inclusive = rows >= cols
     strict = rows > cols
-    cumulative = mm(inclusive.astype(jnp.float32).astype(jnp.bfloat16), log_decay, 3)
-    middle = cumulative[T // 2 : T // 2 + 1, :]
-    final = cumulative[T - 1 : T, :]
-    forward = jnp.exp(cumulative - middle)
-    backward = jnp.exp(middle - cumulative)
-    tail = jnp.exp(final - cumulative)
-    queries = jnp.concatenate([left * jnp.exp(-log_decay) * forward, q * forward], axis=0)
-    sources = jnp.concatenate([right * backward, k * backward], axis=0)
-    start_target = left * jnp.exp(cumulative - log_decay)
-    right_tail = right * tail
-    key_tail = k * tail
+    running = inclusive.astype(jnp.float32).astype(jnp.bfloat16)
     eye = lax.broadcasted_iota(jnp.int32, (LANES, LANES), 0) == lax.broadcasted_iota(
         jnp.int32, (LANES, LANES), 1
     )
-    transit = jnp.where(eye, jnp.exp(final), 0.0)
-    start_read = q * jnp.exp(cumulative)
-    added = jnp.zeros((LANES, LANES), jnp.float32)
-    local_out = jnp.zeros((T, LANES), jnp.float32)
-    lane = lax.broadcasted_iota(jnp.int32, (1, LANES), 1) // width
-    for head in range(LANES // width):
-        only = lane == head
-        pick = (lambda a: a) if width == LANES else (lambda a: jnp.where(only, a, 0.0))
-        pairs = mm_nt(pick(queries), sources)
-        remove_remove = jnp.where(strict, pairs[:T, :T], 0.0)
+    decays = [t[5] - jnp.exp(jnp.float32(-0.5)) * sigmoid(t[3].astype(jnp.float32)) for t in tokens]
+    cumulatives = [mm(running, d, 3) for d in decays]
+    heads, units = [], []
+    for width, (q, k, v, fade, speed, extra), log_decay, cumulative in zip(
+        widths, tokens, decays, cumulatives
+    ):
+        q, k = q.astype(jnp.float32), k.astype(jnp.float32)
+        removal = k * lax.rsqrt(mm(k * k, same_head(width)) + key_epsilon)
+        left = -removal
+        right = sigmoid(speed.astype(jnp.float32)) * removal
+        middle = cumulative[T // 2 : T // 2 + 1, :]
+        final = cumulative[T - 1 : T, :]
+        forward = jnp.exp(cumulative - middle)
+        backward = jnp.exp(middle - cumulative)
+        tail = jnp.exp(final - cumulative)
+        queries = split(jnp.concatenate([left * jnp.exp(-log_decay) * forward, q * forward], axis=0))
+        sources = split(jnp.concatenate([right * backward, k * backward], axis=0))
+        start_target = left * jnp.exp(cumulative - log_decay)
+        right_tail = split(right * tail)
+        key_tail = split(k * tail)
+        units.append([
+            jnp.zeros((T, LANES), jnp.float32),
+            q * jnp.exp(cumulative),
+            jnp.where(eye, jnp.exp(final), 0.0),
+            jnp.zeros((LANES, LANES), jnp.float32),
+        ])
+        lane = lax.broadcasted_iota(jnp.int32, (1, LANES), 1) // width
+        for head in range(LANES // width):
+            if width == LANES:
+                pick = lambda a: a
+            else:
+                pick = lambda a, only=lane == head: jnp.where(only, a, jnp.zeros_like(a))
+            heads.append((
+                len(units) - 1, pick(v), pick(start_target), [pick(x) for x in right_tail],
+                [pick(x) for x in key_tail],
+                product_of([pick(x) for x in queries], sources, NT),
+            ))
+    inverses = unit_inverses(
+        [jnp.where(strict, h[5][:T, :T], 0.0) for h in heads], rows, cols
+    )
+    for (u, value, target, head_right, head_key, pairs), inverse in zip(heads, inverses):
         remove_key = jnp.where(strict, pairs[:T, T:], 0.0)
         read_remove = jnp.where(inclusive, pairs[T:, :T], 0.0)
         read_key = jnp.where(inclusive, pairs[T:, T:], 0.0)
-        inverse = unit_inverse(remove_remove, rows, cols)
-        value = pick(v)
-        carried = mm(inverse, mm(remove_key, value))
-        start = mm(inverse, pick(start_target))
-        local_out = local_out + mm(read_remove, carried) + mm(read_key, value)
-        start_read = start_read + mm(read_remove, start)
-        head_right = pick(right_tail)
-        transit = transit + mm(start.T, head_right)
-        added = added + mm(carried.T, head_right) + mm(value.T, pick(key_tail))
-    return local_out, start_read, transit, added
+        both = mm(inverse, jnp.concatenate([mm(remove_key, value), target], axis=1))
+        reads = mm(read_remove, both)
+        moved = product_of(split(both), head_right, TN)
+        units[u][0] = units[u][0] + reads[:, :LANES] + mm(read_key, value)
+        units[u][1] = units[u][1] + reads[:, LANES:]
+        units[u][2] = units[u][2] + moved[LANES:]
+        units[u][3] = units[u][3] + moved[:LANES] + product_of([value], head_key, TN)
+    return units
 
 
 def finish_unit(width, read, q, k, v, gain, own, gate):
@@ -148,7 +193,7 @@
     residual_ref, scale_ref, project_hbm, gate_hbm, up_hbm, down_hbm,
     out_ref,
     local_ref, read_ref, near, total_move, total_add, chain_in, chain_out, mixed_ref, project,
-    wide, tall, pair_send, pair_got, term_send, term_got, hidden, active, summed,
+    total, wide, tall, pair_send, pair_got, term_send, term_got, hidden, active, summed,
     low_send, low_got, high_send, high_got, line_send, line_got,
     project_sem, keep_sem, out_sem, in_sem, pass_out, pass_in,
     near_out, near_in, chain_sem_out, chain_sem_in, pair_out, pair_in, term_out, term_in,
@@ -265,15 +310,22 @@
 
             guarded(part, m, begin)
 
-    def send_weight(w, chosen_parts):
+    def send_part(w, part, d, upward):
+        dest = member(d)
+        chosen = dest > m if upward else dest < m
+        if part:
+            chosen = chosen & more(dest)
+        pl.when(chosen)(lambda: give(w, part, d).start())
+
+    def send_weight(w, upward, chosen_parts):
         for part in chosen_parts:
-            for upward, ways in ((True, range(F - 1, 0, -1)), (False, range(1, F))):
-                for d in ways:
-                    dest = member(d)
-                    chosen = dest > m if upward else dest < m
-                    if part:
-                        chosen = chosen & more(dest)
-                    pl.when(chosen)(lambda: give(w, part, d).start())
+            for d in range(F - 1, 0, -1) if upward else range(1, F):
+                send_part(w, part, d, upward)
+
+    def send_near_first(w, upward, chosen_parts):
+        for d in range(1, F) if upward else range(F - 1, 0, -1):
+            for part in chosen_parts:
+                send_part(w, part, d, upward)
 
     def relay_weight(w, chosen_parts):
         for part in chosen_parts:
@@ -297,9 +349,12 @@
 
             guarded(part, m, settle)
 
-    for w in range(2):
-        open_weight(w)
-        send_weight(w, range(parts))
+    every, first, rest = range(parts), range(1), range(1, parts)
+    open_weight(0)
+    send_weight(0, True, every)
+    send_weight(0, False, every)
+    send_weight(1, False, every)
+    send_weight(2, False, first)
     if extra:
 
         @pl.when(jnp.logical_not(more(m)))
@@ -327,11 +382,12 @@
             near_in.at[u, e], me, t,
         )
 
-    for u, (group, c) in enumerate(units):
-        local_out, start_read, transit, added = local_unit(
-            widths[group],
-            *(load(r, group, c) for r in (q_ref, k_ref, v_ref, f_ref, a_ref, e_ref)),
-        )
+    def blocks(group, c):
+        lanes = slice(c * LANES, (c + 1) * LANES)
+        return [r[group, :, lanes] for r in (q_ref, k_ref, v_ref, f_ref, a_ref, e_ref)]
+
+    local = local_units([widths[group] for group, _ in units], [blocks(*unit) for unit in units])
+    for u, (local_out, start_read, transit, added) in enumerate(local):
         local_ref[u] = local_out
         read_ref[u] = start_read
         near[g, u, 0] = transit.astype(jnp.bfloat16)
@@ -344,7 +400,8 @@
     def _():
         chain_in[...] = jnp.zeros_like(chain_in)
 
-    relay_weight(0, range(parts))
+    open_weight(1)
+    open_weight(2)
 
     def chain_copy(u):
         return remote(
@@ -374,6 +431,10 @@
         @pl.when(m < F - 1)
         def _():
             chain_copy(u).start()
+
+    send_near_first(1, True, every)
+    send_near_first(2, True, first)
+    relay_weight(0, range(parts))
 
     def fold(other_g, states):
         return tuple(
@@ -426,7 +487,6 @@
         if h:
             term_send[h] = branch.astype(jnp.bfloat16)
             term_copy(h).start()
-    relay_weight(1, range(parts))
     for h in range(1, HI):
         term_copy(h).wait_recv()
         branch = branch + term_got[h].astype(jnp.float32)
@@ -486,44 +546,17 @@
     for d in range(1, F):
         pl.when(m + d >= F)(lambda: row_copy(m, d).start())
     spread(m)
-    open_weight(2)
-    send_weight(2, range(parts))
-
-    @pl.loop(0, F + 2)
-    def _(i):
-        @pl.when((i < F) & (i != m))
-        def _():
-            row_copy(i, 0).wait_recv()
-            spread(i)
-
-        @pl.when((i >= 1) & (i <= F))
-        def _():
-            for h in range(1, HI):
-                up_take(i - 1, h).wait_recv()
-                for l in range(1, LO):
-                    side_copy(i - 1, h, l).start()
-
-        @pl.when(i == 2)
-        def _():
-            arrived_weight(0)
-            arrived_weight(1)
-
-        @pl.when(i >= 2)
-        def _():
-            for h in range(HI):
-                for l in range(1, LO):
-                    side_take(i - 2, h, l).wait_recv()
-            activate(i - 2)
-
-    relay_weight(2, range(parts))
-    arrived_weight(2)
+    send_weight(2, True, rest)
+    send_weight(2, False, rest)
+    relay_weight(1, range(parts))
+
+    def turn(k):
+        return jnp.where(k == 0, m, k - 1 + (k - 1 >= m).astype(jnp.int32))
 
     def target(k):
-        if k == F - 1:
-            return m
         rising = k + (k >= m).astype(jnp.int32)
         falling = F - 1 - k - (F - 1 - k <= m).astype(jnp.int32)
-        return jnp.where(2 * m >= F, rising, falling)
+        return jnp.where(k == F - 1, m, jnp.where(2 * m >= F, rising, falling))
 
     def low_copy(k, h, l):
         return remote(
@@ -539,14 +572,25 @@
 
     def line_copy(k):
         return remote(
-            line_send.at[k], line_got.at[m], line_out.at[k], line_in.at[m],
-            target(k) * T + g, t,
+            line_send.at[k], line_got.at[m], line_out.at[k], line_in.at[m], target(k) * T + g, t
         )
 
     def line_take(a):
         return remote(line_send.at[0], line_got.at[a], line_out.at[0], line_in.at[a], me, t)
 
-    for k in range(F):
+    def across(k):
+        for h in range(1, HI):
+            up_take(turn(k), h).wait_recv()
+            for l in range(1, LO):
+                side_copy(turn(k), h, l).start()
+
+    def gathered(k):
+        for h in range(HI):
+            for l in range(1, LO):
+                side_take(turn(k), h, l).wait_recv()
+        activate(turn(k))
+
+    def contract(k):
         here = positions(target(k))
         units_here = active[here, :]
         for s in range(n_sp):
@@ -564,7 +608,7 @@
             value = value + low_got[k, h, l].astype(jnp.float32)
         return value
 
-    for k in range(F):
+    def halve(k):
         for h in range(HI):
             for l in range(1, LO):
                 low_copy(k, h, l).wait_recv()
@@ -572,24 +616,60 @@
             high_send[k, h] = two_cores(k, h).astype(jnp.bfloat16)
             high_copy(k, h).start()
 
-    for k in range(F):
+    def whole(k):
         value = two_cores(k, 0)
         for h in range(1, HI):
             high_copy(k, h).wait_recv()
             value = value + high_got[k, h].astype(jnp.float32)
-        if k < F - 1:
-            line_send[k] = value.astype(jnp.bfloat16)
-            line_copy(k).start()
-    summed[:tokens, :own_cols] = hidden[positions(m), columns(t)].astype(jnp.float32) + value
+        return value
+
+    relay_weight(2, range(1))
+    across(0)
+
+    @pl.loop(1, F + 1)
+    def _(i):
+        @pl.when(i < F)
+        def _():
+            row_copy(turn(i), 0).wait_recv()
+            spread(turn(i))
+
+        @pl.when(i >= 2)
+        def _():
+            across(i - 1)
+
+    relay_weight(2, range(1, parts))
+    arrived_weight(0)
+    arrived_weight(1)
+
+    @pl.loop(0, F)
+    def _(k):
+        gathered(k)
+
+    arrived_weight(2)
+
+    @pl.loop(0, F)
+    def _(k):
+        contract(k)
+
+    @pl.loop(0, F)
+    def _(k):
+        halve(k)
+
+    @pl.loop(0, F - 1)
+    def _(k):
+        line_send[k] = whole(k).astype(jnp.bfloat16)
+        line_copy(k).start()
+
+    total[...] = hidden[positions(m), columns(t)].astype(jnp.float32) + whole(F - 1)
 
     @pl.loop(0, F)
     def _(a):
         @pl.when(a != m)
         def _():
             line_take(a).wait_recv()
-            summed[:tokens, :own_cols] += line_got[a].astype(jnp.float32)
-
-    out_ref[...] = summed[:tokens, :own_cols].astype(jnp.bfloat16)
+            total[...] += line_got[a].astype(jnp.float32)
+
+    out_ref[...] = total[...].astype(jnp.bfloat16)
 
     for w in range(3):
         for part in range(parts):
@@ -653,6 +733,7 @@
         pltpu.VMEM((units, LANES, LANES), bf16),
         pltpu.VMEM((tokens, units * LANES), bf16),
         pltpu.VMEM(project.shape, bf16),
+        pltpu.VMEM((tokens, cols), f32),
         pltpu.VMEM((2, depth, width), bf16),
         pltpu.VMEM((n_sp, width, down.shape[1]), bf16),
         pltpu.VMEM((HI, LO, tokens, cols), bf16),

time: 109 us -> 99.5 us (0.913)
  Pallas kernels: 108 us -> 97.8 us
    pallas_call x1, Pallas kernels: 108 us -> 97.8 us  [layer(): pl.pallas_call(functools.partial(layer_kernel, n_sp, n_tp, (DS, DL)), out...]
where the time goes in v3:
time: 99.5 us; the launch traced here: 99.4 us
  Pallas kernels  97.8 us (98%)
  local copies, waits for them, and re-layouts  1.57 us (2%)
    pallas_call x1, Pallas kernels, layer(): pl.pallas_call(functools.partial(layer_kernel, n_sp, n_tp, (DS, DL)), out...  97.8 us

profile of v3, /device:TPU:0, one launch (start us, length us, event | category | flops | bytes accessed | tf_op | source)
XLA Modules:
  0.0 99.4 jit_solution(471480676854178712)
XLA Ops:
  0.0 97.8 %layer.1 = bf16[128,512]{1,0:T(8,128)(2,1)} custom-call(bf16[2,128,256]{2,1,0:T(8,128)(2,1)} %q_ref.1, bf16[2,128,256]{2,1,0:T(8,128)(2,1)} %k_ref.1, bf16[2,128,256]{2,1,0:T(8,128)(2,1)} %v_ref.1, bf16[2,128,256]{2,1,0:T(8,128)(2,1)} %f_ref.1, bf16[2,128,256]{2,1,0:T(8,128)(2,1)} %a_ref.1, f32[2,128,256]{2,1,0:T(8,128)} %e_ref.1, ...), custom_call_target="tpu_custom_call" | custom-call | tf_op jit(solution)/shard_map/layer/pallas_call | solution.py:759
  97.8 1.6 %copy.17 = bf16[128,512]{1,0:T(8,128)(2,1)} copy(bf16[128,512]{1,0:T(8,128)(2,1)} %layer.1) | data formatting | bytes 262144

commit v4 on v3

--- a/solution.py
+++ b/solution.py
@@ -198,7 +198,7 @@
     project_sem, keep_sem, out_sem, in_sem, pass_out, pass_in,
     near_out, near_in, chain_sem_out, chain_sem_in, pair_out, pair_in, term_out, term_in,
     row_out, row_in, up_out, up_in, side_out, side_in,
-    low_out, low_in, high_out, high_in, line_out, line_in,
+    low_out, low_in, high_out, high_in, line_out, line_in, mate_out,
 ):
     F = members_of(n_sp)
     T = n_sp // F
@@ -505,6 +505,18 @@
             block(a, t), block(a, t), row_out.at[d], row_in.at[a], member(d) * T + g, t
         )
 
+    def nearer(b, a):
+        return (b // 2 == a // 2) | ((a > b) == (b % 2 == 1)) | (F % 2 == 1)
+
+    def mate_copy(a):
+        return remote(
+            block(a, t), block(a, t), mate_out.at[a], row_in.at[a],
+            (m + 1 - 2 * (m % 2)) * T + g, t,
+        )
+
+    def hands_on(a):
+        return nearer(m, a) & (a // 2 != m // 2) & (F % 2 == 0)
+
     def up_copy(a, h):
         return remote(block(a, t), block(a, t), up_out.at[a, h], up_in.at[a, h], me, cell(h, 0))
 
@@ -542,9 +554,9 @@
         active[positions(a), :] = value.astype(jnp.bfloat16)
 
     for d in range(1, F):
-        pl.when(m + d < F)(lambda: row_copy(m, d).start())
+        pl.when((m + d < F) & nearer(member(d), m))(lambda: row_copy(m, d).start())
     for d in range(1, F):
-        pl.when(m + d >= F)(lambda: row_copy(m, d).start())
+        pl.when((m + d >= F) & nearer(member(d), m))(lambda: row_copy(m, d).start())
     spread(m)
     send_weight(2, True, rest)
     send_weight(2, False, rest)
@@ -623,7 +635,6 @@
             value = value + high_got[k, h].astype(jnp.float32)
         return value
 
-    relay_weight(2, range(1))
     across(0)
 
     @pl.loop(1, F + 1)
@@ -631,17 +642,31 @@
         @pl.when(i < F)
         def _():
             row_copy(turn(i), 0).wait_recv()
+            pl.when(hands_on(turn(i)))(lambda: mate_copy(turn(i)).start())
             spread(turn(i))
+
+            @pl.when(i == 1)
+            def _():
+                relay_weight(2, first)
+
+            @pl.when(i == F - 1)
+            def _():
+                relay_weight(2, rest)
 
         @pl.when(i >= 2)
         def _():
             across(i - 1)
 
-    relay_weight(2, range(1, parts))
-    arrived_weight(0)
-    arrived_weight(1)
-
-    @pl.loop(0, F)
+        @pl.when(i == 2)
+        def _():
+            arrived_weight(0)
+            arrived_weight(1)
+
+        @pl.when(i >= 3)
+        def _():
+            gathered(i - 3)
+
+    @pl.loop(max(F - 2, 0), F)
     def _(k):
         gathered(k)
 
@@ -698,8 +723,9 @@
             pair_copy(h, l).wait_send()
     for d in range(F):
         if d:
-            row_copy(m, d).wait_send()
+            pl.when(nearer(member(d), m))(lambda: row_copy(m, d).wait_send())
             line_copy(d - 1).wait_send()
+        pl.when(hands_on(d))(lambda: mate_copy(d).wait_send())
         for h in range(HI):
             if h:
                 up_copy(d, h).wait_send()
@@ -756,6 +782,7 @@
         (F, HI, LO), (F, HI), (F,),
     ):
         scratch += [sem(shape), sem(shape)]
+    scratch.append(sem((F,)))
     return pl.pallas_call(
         functools.partial(layer_kernel, n_sp, n_tp, (DS, DL)),
         out_shape=jax.ShapeDtypeStruct((tokens, cols), bf16),

time: 99.5 us -> 94.5 us (0.950)
  Pallas kernels: 97.8 us -> 92.4 us
    pallas_call x1, Pallas kernels: 97.8 us -> 92.4 us  [layer(): pl.pallas_call(functools.partial(layer_kernel, n_sp, n_tp, (DS, DL)), out...]
where the time goes in v4:
time: 94.5 us; the launch traced here: 94 us
  Pallas kernels  92.4 us (98%)
  local copies, waits for them, and re-layouts  1.57 us (2%)
    pallas_call x1, Pallas kernels, layer(): pl.pallas_call(functools.partial(layer_kernel, n_sp, n_tp, (DS, DL)), out...  92.4 us

profile of v4, /device:TPU:0, one launch (start us, length us, event | category | flops | bytes accessed | tf_op | source)
XLA Modules:
  0.0 94.0 jit_solution(1289142440647647910)
XLA Ops:
  0.0 92.4 %layer.1 = bf16[128,512]{1,0:T(8,128)(2,1)} custom-call(bf16[2,128,256]{2,1,0:T(8,128)(2,1)} %q_ref.1, bf16[2,128,256]{2,1,0:T(8,128)(2,1)} %k_ref.1, bf16[2,128,256]{2,1,0:T(8,128)(2,1)} %v_ref.1, bf16[2,128,256]{2,1,0:T(8,128)(2,1)} %f_ref.1, bf16[2,128,256]{2,1,0:T(8,128)(2,1)} %a_ref.1, f32[2,128,256]{2,1,0:T(8,128)} %e_ref.1, ...), custom_call_target="tpu_custom_call" | custom-call | tf_op jit(solution)/shard_map/layer/pallas_call | solution.py:786
  92.4 1.6 %copy.17 = bf16[128,512]{1,0:T(8,128)(2,1)} copy(bf16[128,512]{1,0:T(8,128)(2,1)} %layer.1) | data formatting | bytes 262144

commit v5 on v4

--- a/solution.py
+++ b/solution.py
@@ -370,15 +370,33 @@
 
     units = [(group, c) for group in range(2) for c in range(per_group)]
 
+    def own_rows(u):
+        return pl.ds(0, widths[units[u][0]])
+
+    def pack(u, x):
+        width = widths[units[u][0]]
+        return sum(x[at : at + width] for at in range(0, LANES, width)).astype(jnp.bfloat16)
+
+    def unpack(u, x):
+        width = widths[units[u][0]]
+        if width == LANES:
+            return x
+        return jnp.concatenate([x] * (LANES // width), axis=0) * same_head(width)
+
+    def near_state(source_g, u, i):
+        return unpack(u, near[source_g, u, i, own_rows(u), :])
+
     def near_copy(u, e):
-        return remote(
-            near.at[g, u], near.at[g, u], near_out.at[u, e], near_in.at[u, e],
+        at = near.at[g, u, :, own_rows(u)]
+        return remote(
+            at, at, near_out.at[u, e], near_in.at[u, e],
             m * T + other(e), t,
         )
 
     def near_take(u, e):
-        return remote(
-            near.at[other(-e), u], near.at[other(-e), u], near_out.at[u, e],
+        at = near.at[other(-e), u, :, own_rows(u)]
+        return remote(
+            at, at, near_out.at[u, e],
             near_in.at[u, e], me, t,
         )
 
@@ -390,8 +408,8 @@
     for u, (local_out, start_read, transit, added) in enumerate(local):
         local_ref[u] = local_out
         read_ref[u] = start_read
-        near[g, u, 0] = transit.astype(jnp.bfloat16)
-        near[g, u, 1] = added.astype(jnp.bfloat16)
+        near[g, u, 0, own_rows(u), :] = pack(u, transit)
+        near[g, u, 1, own_rows(u), :] = pack(u, added)
     for u in range(len(units)):
         for e in range(1, T):
             near_copy(u, e).start()
@@ -405,17 +423,17 @@
 
     def chain_copy(u):
         return remote(
-            chain_out.at[u], chain_in.at[u], chain_sem_out.at[u], chain_sem_in.at[u],
+            chain_out.at[u, own_rows(u)], chain_in.at[u, own_rows(u)], chain_sem_out.at[u], chain_sem_in.at[u],
             member(1) * T + g, t,
         )
 
     for u in range(len(units)):
         for e in range(1, T):
             near_take(u, e).wait_recv()
-        move, add = near[0, u, 0], near[0, u, 1].astype(jnp.float32)
+        move, add = near_state(0, u, 0), near_state(0, u, 1).astype(jnp.float32)
         for other_g in range(1, T):
-            step = near[other_g, u, 0]
-            add = mm(add, step) + near[other_g, u, 1].astype(jnp.float32)
+            step = near_state(other_g, u, 0)
+            add = mm(add, step) + near_state(other_g, u, 1).astype(jnp.float32)
             move = mm(move, step).astype(jnp.bfloat16)
         total_move[u] = move
         total_add[u] = add
@@ -425,8 +443,8 @@
         def _():
             chain_copy(u).wait_recv()
 
-        following = mm(chain_in[u], total_move[u]) + total_add[u]
-        chain_out[u] = following.astype(jnp.bfloat16)
+        before = unpack(u, chain_in[u, own_rows(u), :])
+        chain_out[u, own_rows(u), :] = pack(u, mm(before, total_move[u]) + total_add[u])
 
         @pl.when(m < F - 1)
         def _():
@@ -438,12 +456,14 @@
 
     def fold(other_g, states):
         return tuple(
-            mm(s, near[other_g, u, 0]) + near[other_g, u, 1].astype(jnp.float32)
+            mm(s, near_state(other_g, u, 0)) + near_state(other_g, u, 1).astype(jnp.float32)
             for u, s in enumerate(states)
         )
 
     states = lax.fori_loop(
-        0, g, fold, tuple(chain_in[u].astype(jnp.float32) for u in range(len(units)))
+        0, g, fold, tuple(
+            unpack(u, chain_in[u, own_rows(u), :]).astype(jnp.float32) for u in range(len(units))
+        )
     )
     for u, (group, c) in enumerate(units):
         lanes = slice(c * LANES, (c + 1) * LANES)

time: 94.5 us -> 93.1 us (0.985)
  Pallas kernels: 92.4 us -> 91.3 us
    pallas_call x1, Pallas kernels: 92.4 us -> 91.3 us  [layer(): pl.pallas_call(functools.partial(layer_kernel, n_sp, n_tp, (DS, DL)), out...]
where the time goes in v5:
time: 93.1 us; the launch traced here: 92.9 us
  Pallas kernels  91.3 us (98%)
  local copies, waits for them, and re-layouts  1.57 us (2%)
    pallas_call x1, Pallas kernels, layer(): pl.pallas_call(functools.partial(layer_kernel, n_sp, n_tp, (DS, DL)), out...  91.3 us

profile of v5, /device:TPU:0, one launch (start us, length us, event | category | flops | bytes accessed | tf_op | source)
XLA Modules:
  0.0 92.9 jit_solution(15113685950797482744)
XLA Ops:
  0.0 91.3 %layer.1 = bf16[128,512]{1,0:T(8,128)(2,1)} custom-call(bf16[2,128,256]{2,1,0:T(8,128)(2,1)} %q_ref.1, bf16[2,128,256]{2,1,0:T(8,128)(2,1)} %k_ref.1, bf16[2,128,256]{2,1,0:T(8,128)(2,1)} %v_ref.1, bf16[2,128,256]{2,1,0:T(8,128)(2,1)} %f_ref.1, bf16[2,128,256]{2,1,0:T(8,128)(2,1)} %a_ref.1, f32[2,128,256]{2,1,0:T(8,128)} %e_ref.1, ...), custom_call_target="tpu_custom_call" | custom-call | tf_op jit(solution)/shard_map/layer/pallas_call | solution.py:806
  91.4 1.6 %copy.17 = bf16[128,512]{1,0:T(8,128)(2,1)} copy(bf16[128,512]{1,0:T(8,128)(2,1)} %layer.1) | data formatting | bytes 262144
